TPU v7x, 32 devices: a whole 2x2x4 slice. The times are simulated.
32 devices in a mesh: sp: 16 (over z, y, x), tp: 2 (over core).
Axes of the slice: x: 2, y: 2, z: 4, core: 2. Of those that a mesh axis runs over, the one named last changes fastest.
Arguments:
- queries: bfloat16 [8192, 2048], P('sp', 'tp'), may hold values from -6 to 6
- keys: bfloat16 [8192, 1024], P('sp', 'tp'), may hold values from -6 to 6
- values: bfloat16 [8192, 1024], P('sp', 'tp'), may hold values from -6 to 6
- documents: int32 [8192], P('sp'), may hold values from 0 to 3, never falling along the last dimension, each value on 1 to 4096 neighbouring positions
- query_gain: float32 [128], replicated, may hold values from 1.8 to 6
- key_gain: float32 [128], replicated, may hold values from 1.8 to 6
- residual: bfloat16 [8192, 4096], P('sp', 'tp'), may hold values from -6 to 6
- out_weight: bfloat16 [2048, 4096], P('tp'), may hold values from -0.125 to 0.125
- norm_gain: float32 [4096], replicated, may hold values from 0.1 to 1.9
- up_weight: bfloat16 [4096, 16384], P('sp', 'tp'), may hold values from -0.09375 to 0.09375
- down_weight: bfloat16 [16384, 4096], P('tp', 'sp'), may hold values from -0.046875 to 0.046875
Outputs:
- mixed: bfloat16 [8192, 4096], P('sp', 'tp')
Inputs may be any that keep to these rules, and one draw needn't show every extreme that they name: `documents`: document numbers never fall along the sequence; a document has at most 4096 positions.
All inputs are finite; a program needn't handle non-finite values.
Results may differ from a plain program's by a relative error of at most 0.017.
The roundings to bfloat16 on the way count: a program that leaves them out, or rounds other values in their place, can miss the bound.
Values may be sent and summed in bfloat16 or wider, within the bound.
No kernel may reach another device: no remote copies, remote signals or barrier semaphores. Data moves between devices by JAX's collectives and lax.ppermute only.
A program may use at most 256 MiB of HBM per device.

v0:
```python
import jax
import jax.numpy as jnp
from jax import lax
from jax.sharding import PartitionSpec as P

HQ = 16
KV = 8
HD = 128
GRID_W = 64


norm_eps = 1e-06
rope_base = 10000.0
masked_score = -1e30


def head_norm(heads_in, gain):
    values32 = heads_in.astype(jnp.float32)
    scaled = values32 * lax.rsqrt(jnp.mean(values32 * values32, axis=-1, keepdims=True) + norm_eps)
    return scaled * gain


def rotate_half(heads_in, position):
    quarter = heads_in.shape[-1] // 2
    inverse_freq = rope_base ** (-jnp.arange(quarter, dtype=jnp.float32) / quarter)
    angles = position[:, None] * inverse_freq[None, :]
    cosine_part = jnp.cos(angles)[:, None, :]
    sine_part = jnp.sin(angles)[:, None, :]
    leading = heads_in[..., :quarter]
    trailing = heads_in[..., quarter:]
    return jnp.concatenate(
        [
            leading * cosine_part - trailing * sine_part,
            leading * sine_part + trailing * cosine_part,
        ],
        axis=-1,
    )


def grid_rotary(heads_in, positions):
    half_width = heads_in.shape[-1] // 2
    grid_row = (positions // GRID_W).astype(jnp.float32)
    grid_col = (positions % GRID_W).astype(jnp.float32)
    return jnp.concatenate(
        [
            rotate_half(heads_in[..., :half_width], grid_row),
            rotate_half(heads_in[..., half_width:], grid_col),
        ],
        axis=-1,
    )


def body(
    queries,
    keys,
    values,
    documents,
    query_gain,
    key_gain,
    residual,
    out_weight,
    norm_gain,
    up_weight,
    down_weight,
):
    tok_rows = queries.shape[0]
    key_heads = keys.shape[1] // HD
    group_size = HQ // KV
    width_local = residual.shape[1]
    tp_index = lax.axis_index("tp")
    up_whole, down_whole = (
        lax.all_gather(up_weight, "sp", axis=0, tiled=True),
        lax.all_gather(down_weight, "sp", axis=1, tiled=True),
    )
    residual_whole = lax.all_gather(residual, "tp", axis=1, tiled=True)
    positions = lax.axis_index("sp") * tok_rows + jnp.arange(tok_rows, dtype=jnp.int32)
    queries_rot = grid_rotary(
        head_norm(queries.reshape(tok_rows, key_heads * group_size, HD), query_gain), positions
    )
    queries_rot = queries_rot.astype(jnp.bfloat16).reshape(tok_rows, key_heads, group_size, HD)
    keys_rot = grid_rotary(
        head_norm(keys.reshape(tok_rows, key_heads, HD), key_gain), positions
    ).astype(jnp.bfloat16)
    value_heads = values.reshape(tok_rows, key_heads, HD)
    own_docs = documents.astype(jnp.bfloat16)
    score_scale = HD ** (-0.5)
    running_max = jnp.full((key_heads, group_size, tok_rows), masked_score, jnp.float32)
    key_piece = lax.all_gather(keys_rot, "sp", axis=0, tiled=True)
    value_piece = lax.all_gather(value_heads, "sp", axis=0, tiled=True)
    doc_piece = lax.all_gather(own_docs, "sp", axis=0, tiled=True)
    scores = (
        jnp.einsum("qkgd,skd->kgqs", queries_rot, key_piece, preferred_element_type=jnp.float32)
        * score_scale
    )
    same_doc = own_docs[:, None] == doc_piece[None, :]
    scores = jnp.where(same_doc, scores, masked_score)
    new_max = jnp.maximum(running_max, jnp.max(scores, axis=-1))
    probs = jnp.where(same_doc, jnp.exp(scores - new_max[..., None]), 0.0)
    running_sum = jnp.sum(probs, axis=-1)
    update = jnp.einsum(
        "kgqs,skd->qkgd",
        probs.astype(jnp.bfloat16),
        value_piece,
        preferred_element_type=jnp.float32,
    )
    weighted = update
    running_max, running_sum, weighted = (new_max, running_sum, weighted)
    attended = (weighted / jnp.transpose(running_sum, (2, 0, 1))[..., None]).astype(jnp.bfloat16)
    attended = attended.reshape(tok_rows, key_heads * group_size * HD)
    partial_out = jnp.dot(attended, out_weight, preferred_element_type=jnp.float32)
    branch = lax.psum(partial_out.astype(jnp.bfloat16), "tp").astype(jnp.float32)
    stream_whole = residual_whole.astype(jnp.float32) + branch
    normed = stream_whole * lax.rsqrt(
        jnp.mean(stream_whole * stream_whole, axis=-1, keepdims=True) + norm_eps
    )
    normed = (normed * norm_gain).astype(jnp.bfloat16)
    stream = lax.dynamic_slice_in_dim(stream_whole, tp_index * width_local, width_local, 1)
    hidden = jnp.dot(normed, up_whole, preferred_element_type=jnp.float32)
    positive = jnp.maximum(hidden, 0.0)
    squared = (positive * positive).astype(jnp.bfloat16)
    product = jnp.dot(squared, down_whole, preferred_element_type=jnp.float32)
    feed = lax.psum_scatter(
        product.astype(jnp.bfloat16), "tp", scatter_dimension=1, tiled=True
    ).astype(jnp.float32)
    return (stream + feed).astype(jnp.bfloat16)


def solution(mesh):
    in_specs = (
        P("sp", "tp"),
        P("sp", "tp"),
        P("sp", "tp"),
        P("sp"),
        P(),
        P(),
        P("sp", "tp"),
        P("tp", None),
        P(),
        P("sp", "tp"),
        P("tp", "sp"),
    )
    out_specs = P("sp", "tp")
    return jax.shard_map(body, mesh=mesh, in_specs=in_specs, out_specs=out_specs, check_vma=False)
```

profile of v0, /device:TPU:0, one launch (start us, length us, event | category | flops | bytes accessed | tf_op | source)
XLA Modules:
  0.0 2437.9 jit_solution(14920959515710849771)
XLA Ops:
  6.6 1.3 copy.28
  8.0 0.2 copy.29
  8.3 1.9 multiply_cosine_fusion.1
  10.1 1.0 multiply_multiply_fusion.1
  11.1 0.9 subtract_convert_fusion.3
  12.1 1.5 pad_maximum_fusion
  13.6 1.0 copy.36
  14.7 0.7 all-gather.7.cloned.1.call-update
  15.5 0.2 convert_bitcast_fusion
  15.7 0.5 copy.42
  16.2 0.6 multiply_reduce_fusion.1
  17.1 0.9 multiply_multiply_fusion
  18.0 1.8 subtract_convert_fusion.1
  20.2 1.1 copy.35
  21.4 54.7 %all-gather = bf16[16,1,512]{2,1,0:T(2,128)(2,1)S(1)} all-gather(bf16[1,1,512]{2,1,0:T(2,128)(2,1)S(1)} %reshape.192), channel_id=1, replica_groups=mesh['sp'=16,'tp'=2] {'sp'}, dimensions={0}, use_global_device_ids=true | all-gather | bytes 17408 | tf_op jit(solution)/shard_map/all_gather | solution.py:90
  76.2 4.0 broadcast_compare_fusion
  80.2 48.9 %all-gather.9.cloned.1.call-done = bf16[8192,4,128]{2,0,1:T(8,128)(2,1)} async-done(((bf16[512,4,128]{2,0,1:T(8,128)(2,1)}), bf16[8192,4,128]{2,0,1:T(8,128)(2,1)}) %all-gather.9.cloned.1.call-update) | async-done | bytes 8388624 | tf_op jit(solution)/shard_map/all_gather | solution.py:88
  129.1 52.2 %fusion = (f32[4,2,512]{2,1,0:T(2,128)S(1)}, f32[4,8192,512,2]{2,1,3,0:T(8,128)}) fusion(pred[512,8192]{0,1:T(8,128)(4,1)} %broadcast_compare_fusion, bf16[512,4,2,32]{3,0,2,1:T(8,128)(2,1)} %bitcast.60, bf16[512,4,2,32]{3,0,2,1:T(8,128)(2,1)S(1)} %bitcast.59, bf16[512,4,2,32]{3,0,2,1:T(8,128)(2,1)S(1)} %bitcast.58, ...), kind=kOutput, calls=%fused_computation.2 | convolution fusion | flops 8694788096 | bytes 147865600 | tf_op jit(solution)/shard_map/qkgd,skd->kgqs/dot_general | solution.py:92
  181.3 43.7 %fusion.1 = f32[4,2,512]{2,1,0:T(2,128)S(1)} fusion(f32[4,8192,512,2]{2,1,3,0:T(8,128)} %get-tuple-element.26, f32[4,2,512]{2,1,0:T(2,128)S(1)} %broadcast_maximum_fusion, pred[512,8192]{0,1:T(8,128)(4,1)} %broadcast_compare_fusion), kind=kLoop, calls=%fused_computation.3 | loop fusion | flops 167768064 | bytes 138444800 | tf_op jit(solution)/shard_map/reduce_sum | solution.py:99
  225.0 25.8 %all-gather.11.cloned.1.call-done = bf16[8192,4,128]{0,2,1:T(8,128)(2,1)} async-done(((bf16[512,4,128]{0,2,1:T(8,128)(2,1)}), bf16[8192,4,128]{0,2,1:T(8,128)(2,1)}) %all-gather.11.cloned.1.call-update) | async-done | bytes 8388624 | tf_op jit(solution)/shard_map/all_gather | solution.py:89
  250.7 51.7 %fusion.11 = bf16[512,4,2,128]{0,3,2,1:T(8,128)(2,1)S(1)} fusion(f32[4,8192,512,2]{2,1,3,0:T(8,128)} %get-tuple-element.26, f32[4,2,512]{2,1,0:T(2,128)S(1)} %broadcast_maximum_fusion, pred[512,8192]{0,1:T(8,128)(4,1)} %broadcast_compare_fusion, bf16[8192,4,128]{0,2,1:T(8,128)(2,1)} %all-gather.11.cloned.1.call-done, f32[512,4,2]{0,2,1:T(2,128)S(1)} %bitcast.63), kind=kOutput, calls=%fused_computation.21 | convolution fusion | flops 8758755328 | bytes 147881984 | tf_op jit(solution)/shard_map/kgqs,skd->qkgd/dot_general | solution.py:100
  302.5 9.5 convolution_convert_fusion.1
  312.1 0.5 all-gather.13.cloned.1.call-update
  312.7 0.5 all-gather.15.cloned.1.call-update
  313.3 25.2 %all-reduce.2.cloned.1.call-done = bf16[512,4096]{1,0:T(8,128)(2,1)} async-done(((bf16[512,4096]{1,0:T(8,128)(2,1)}), bf16[512,4096]{1,0:T(8,128)(2,1)}) %all-reduce.2.cloned.1.call-update) | async-done | bytes 4194320 | tf_op jit(solution)/shard_map/psum | solution.py:111
  338.4 8.0 convert_add_fusion
  346.5 663.9 %all-gather.13.cloned.1.call-done = bf16[4096,8192]{1,0:T(8,128)(2,1)} async-done(((bf16[256,8192]{1,0:T(8,128)(2,1)}), bf16[4096,8192]{1,0:T(8,128)(2,1)}) %all-gather.13.cloned.1.call-update) | async-done | bytes 67108880 | tf_op jit(solution)/shard_map/all_gather | solution.py:72
  1010.4 45.3 %multiply_convert_fusion = bf16[512,8192]{1,0:T(8,128)(2,1)} fusion(bf16[4096,8192]{1,0:T(8,128)(2,1)} %all-gather.13.cloned.1.call-done, f32[4096]{0:T(1024)S(1)} %copy-done.4, f32[512]{0:T(512)S(1)} %add_rsqrt_fusion.2, bf16[512,4096]{1,0:T(8,128)(2,1)} %all-reduce.2.cloned.1.call-done, bf16[512,4096]{1,0:T(8,128)(2,1)} %all-gather.7.cloned.1.call-done), kind=kOutput, calls=%fused_computation.7 | convolution fusion | flops 34384904192 | bytes 83904512 | tf_op jit(solution)/shard_map/dot_general | solution.py:118
  1055.7 1312.2 %all-gather.15.cloned.1.call-done = bf16[8192,4096]{1,0:T(8,128)(2,1)} async-done(((bf16[8192,256]{1,0:T(8,128)(2,1)}), bf16[8192,4096]{1,0:T(8,128)(2,1)}) %all-gather.15.cloned.1.call-update) | async-done | bytes 67108880 | tf_op jit(solution)/shard_map/all_gather | solution.py:73
  2368.0 44.5 %convolution_convert_fusion = bf16[512,4096]{1,0:T(8,128)(2,1)} fusion(bf16[512,8192]{1,0:T(8,128)(2,1)} %multiply_convert_fusion, bf16[8192,4096]{1,0:T(8,128)(2,1)} %all-gather.15.cloned.1.call-done), kind=kOutput, calls=%fused_computation.14 | convolution fusion | flops 34361835520 | bytes 79691776 | tf_op jit(solution)/shard_map/dot_general | solution.py:121
  2412.5 13.3 reduce-scatter.2.cloned.1.call-done
  2425.8 4.8 add_convert_fusion
  (38 shorter events, 1.3 us)
Async XLA Ops:
  6.5 122.5 %all-gather.9.cloned.1.call-start = ((), (), s32[]{:S(2)}) async-start(), calls=%async_computation.2 | async-start | bytes 8912896 | tf_op jit(solution)/shard_map/all_gather | solution.py:88
  6.6 7.0 copy-start.1
  11.1 4.3 copy-start
  12.0 5.1 copy-start.3
  13.6 237.2 %all-gather.11.cloned.1.call-start = ((), (), s32[]{:S(2)}) async-start(), calls=%async_computation.3 | async-start | bytes 8912896 | tf_op jit(solution)/shard_map/all_gather | solution.py:89
  14.7 298.6 %all-gather.7.cloned.1.call-start = ((), (), s32[]{:S(2)}) async-start(), calls=%async_computation.1 | async-start | bytes 6291456 | tf_op jit(solution)/shard_map/all_gather | solution.py:75
  15.4 323.0 %all-reduce.2.cloned.1.call-start = ((), (), s32[]{:S(2)}) async-start(), calls=%async_computation.4 | async-start | bytes 8388608 | tf_op jit(solution)/shard_map/psum | solution.py:111
  18.0 3.4 copy-start.2
  312.0 698.4 %all-gather.13.cloned.1.call-start = ((), (), s32[]{:S(2)}) async-start(), calls=%async_computation.5 | async-start | bytes 71303168 | tf_op jit(solution)/shard_map/all_gather | solution.py:72
  312.6 2055.4 %all-gather.15.cloned.1.call-start = ((), (), s32[]{:S(2)}) async-start(), calls=%async_computation.6 | async-start | bytes 71303168 | tf_op jit(solution)/shard_map/all_gather | solution.py:73
  313.2 697.2 %copy-start.4 = (f32[4096]{0:T(1024)S(1)}, f32[4096]{0:T(1024)}, u32[]{:S(2)}) copy-start(f32[4096]{0:T(1024)} %param.19) | copy-start | bytes 49156
  313.2 2112.6 %reduce-scatter.2.cloned.1.call-start = ((), (), s32[]{:S(2)}) async-start(), calls=%async_computation.7 | async-start | bytes 6291456 | tf_op jit(solution)/shard_map/reduce_scatter | solution.py:122
Sparse Core Ops, SparseCore 0:
  13.7 115.3 all-gather.8
  131.8 118.9 all-gather.10
  252.3 11.8 all-gather.6
  312.1 26.2 all-reduce.1
  341.1 669.3 all-gather.12
  1011.8 1356.1 all-gather.14
  2412.6 13.0 reduce-scatter.1
where the time goes:
time: 2440 us
  waiting for transfers between devices  2090 us (86%)
  matrix products  203 us (8%)
  other arithmetic  69.7 us (3%)
  blocking collectives  54.7 us (2%)
    all_gather x1, waiting for transfers between devices, body(): lax.all_gather(down_weight, 'sp', axis=1, tiled=True)  1310 us
    all_gather x1, waiting for transfers between devices, body(): lax.all_gather(up_weight, 'sp', axis=0, tiled=True)  664 us
    all_gather x1, blocking collectives, body(): doc_piece = lax.all_gather(own_docs, 'sp', axis=0, tiled=True)  54.7 us
    dot_general x1, matrix products, body(): jnp.einsum('qkgd,skd->kgqs', queries_rot, key_piece, preferred_element_ty...  52.2 us
    dot_general x1, matrix products, body(): jnp.einsum('kgqs,skd->qkgd', probs.astype(jnp.bfloat16), value_piece, pre...  51.7 us
    all_gather x1, waiting for transfers between devices, body(): key_piece = lax.all_gather(keys_rot, 'sp', axis=0, tiled=True)  48.9 us
  transfers between devices with their start and end apart: 7, of which 6 were waited for; matrix products, arithmetic and copies ran while one was open for 9% of the time, Pallas kernels for 0%

commit v1 on v0

v1 whole, which is shorter than its diff:
```python
import functools
import jax
import jax.numpy as jnp
from jax import lax
from jax.experimental import pallas as pl
from jax.experimental.pallas import tpu as pltpu
from jax.sharding import PartitionSpec as P


HQ = 16
KV = 8
HD = 128
GRID_W = 64

norm_eps = 1e-06
rope_base = 10000.0
masked_score = -1e30
log2_e = 1.4426950408889634


def head_norm(heads_in, gain):
    values32 = heads_in.astype(jnp.float32)
    scaled = values32 * lax.rsqrt(jnp.mean(values32 * values32, axis=-1, keepdims=True) + norm_eps)
    return scaled * gain


def rotate_half(heads_in, position):
    quarter = heads_in.shape[-1] // 2
    inverse_freq = rope_base ** (-jnp.arange(quarter, dtype=jnp.float32) / quarter)
    angles = position[:, None] * inverse_freq[None, :]
    cosine_part = jnp.cos(angles)[:, None, :]
    sine_part = jnp.sin(angles)[:, None, :]
    leading = heads_in[..., :quarter]
    trailing = heads_in[..., quarter:]
    return jnp.concatenate(
        [
            leading * cosine_part - trailing * sine_part,
            leading * sine_part + trailing * cosine_part,
        ],
        axis=-1,
    )


def grid_rotary(heads_in, positions):
    half_width = heads_in.shape[-1] // 2
    grid_row = (positions // GRID_W).astype(jnp.float32)
    grid_col = (positions % GRID_W).astype(jnp.float32)
    return jnp.concatenate(
        [
            rotate_half(heads_in[..., :half_width], grid_row),
            rotate_half(heads_in[..., half_width:], grid_col),
        ],
        axis=-1,
    )


def attend_kernel(flags, q_ref, kv_ref, qdoc_ref, kdoc_ref, out_ref, max_ref, sum_ref, acc_ref, *, group, blocks):
    tile = pl.program_id(0)
    tokens = q_ref.shape[0]
    factor = log2_e * HD ** (-0.5)
    rows = jnp.concatenate([q_ref[:, g * HD : (g + 1) * HD] for g in range(group)], axis=0)
    max_ref[...] = jnp.full(max_ref.shape, masked_score, jnp.float32)
    sum_ref[...] = jnp.zeros(sum_ref.shape, jnp.float32)
    acc_ref[...] = jnp.zeros(acc_ref.shape, jnp.float32)

    def block_step(block, masked):
        scores = lax.dot_general(
            kv_ref[block, :, :HD], rows, (((1,), (1,)), ((), ())), preferred_element_type=jnp.float32
        )
        if masked:
            same = kdoc_ref[block] == qdoc_ref[0]
            scores = jnp.where(same, scores, masked_score)
        old_max = max_ref[...]
        new_max = jnp.maximum(old_max, jnp.max(scores, axis=0, keepdims=True))
        alpha = jnp.exp2((old_max - new_max) * factor)
        probs = jnp.exp2((scores - new_max) * factor)
        if masked:
            probs = jnp.where(same, probs, 0.0)
        sum_ref[...] = sum_ref[...] * alpha + jnp.sum(probs, axis=0, keepdims=True)
        acc_ref[...] = acc_ref[...] * alpha + lax.dot_general(
            kv_ref[block, :, HD:],
            probs.astype(jnp.bfloat16),
            (((0,), (0,)), ((), ())),
            preferred_element_type=jnp.float32,
        )
        max_ref[...] = new_max

    def loop_body(block, carry):
        kind = flags[tile * blocks + block]

        @pl.when(kind == 1)
        def _():
            block_step(block, True)

        @pl.when(kind == 2)
        def _():
            block_step(block, False)

        return carry

    lax.fori_loop(0, blocks, loop_body, 0)
    result = jnp.transpose(acc_ref[...] / sum_ref[...]).astype(jnp.bfloat16)
    for g in range(group):
        out_ref[:, g * HD : (g + 1) * HD] = result[g * tokens : (g + 1) * tokens]


def attend(q_blocks, kv_blocks, q_docs, kv_docs, group):
    q_count, rows, width = q_blocks.shape
    blocks, block_rows, _ = kv_blocks.shape
    tile_rows = min(256, rows)
    tiles = q_count * rows // tile_rows
    q_flat = q_blocks.reshape(tiles * tile_rows, width)
    q_tiles = q_docs.reshape(tiles, tile_rows)
    low, high = q_tiles[:, :1], q_tiles[:, -1:]
    key_low, key_high = kv_docs[None, :, 0], kv_docs[None, :, -1]
    needed = (key_low <= high) & (key_high >= low)
    whole = (low == high) & (key_low == key_high)
    flags = jnp.where(needed, jnp.where(whole, 2, 1), 0).astype(jnp.int32).reshape(-1)
    grid_spec = pltpu.PrefetchScalarGridSpec(
        num_scalar_prefetch=1,
        grid=(tiles,),
        in_specs=[
            pl.BlockSpec((tile_rows, width), lambda t, f: (t, 0)),
            pl.BlockSpec((blocks, block_rows, 2 * HD), lambda t, f: (0, 0, 0)),
            pl.BlockSpec((1, 1, group * tile_rows), lambda t, f: (t, 0, 0)),
            pl.BlockSpec((blocks, block_rows, 1), lambda t, f: (0, 0, 0)),
        ],
        out_specs=pl.BlockSpec((tile_rows, width), lambda t, f: (t, 0)),
        scratch_shapes=[
            pltpu.VMEM((1, group * tile_rows), jnp.float32),
            pltpu.VMEM((1, group * tile_rows), jnp.float32),
            pltpu.VMEM((HD, group * tile_rows), jnp.float32),
        ],
    )
    pairs = tiles * tile_rows * group * blocks * block_rows
    out = pl.pallas_call(
        functools.partial(attend_kernel, group=group, blocks=blocks),
        grid_spec=grid_spec,
        out_shape=jax.ShapeDtypeStruct(q_flat.shape, jnp.bfloat16),
        cost_estimate=pl.CostEstimate(
            flops=2 * pairs * HD, bytes_accessed=4 * q_flat.size + 2 * kv_blocks.size, transcendentals=pairs // 2
        ),
        name="attend",
    )(flags, q_flat, kv_blocks, jnp.tile(q_tiles, (1, group))[:, None, :], kv_docs[:, :, None])
    return out.reshape(q_blocks.shape)


def up_kernel(part, col, *refs, tp, slots, slab):
    x_refs, w_ref, out_ref, rows_ref = refs[:tp], refs[tp], refs[tp + 1], refs[tp + 2]

    @pl.when(pl.program_id(0) == 0)
    def _():
        for s in range(slots):
            for j in range(tp):

                @pl.when(part[s] == j)
                def _(s=s, j=j):
                    at = pl.multiple_of(col[s], slab)
                    rows_ref[:, s * slab : (s + 1) * slab] = x_refs[j][:, pl.ds(at, slab)]

    hidden = jnp.dot(rows_ref[...], w_ref[...], preferred_element_type=jnp.float32)
    positive = jnp.maximum(hidden, 0.0)
    out_ref[...] = (positive * positive).astype(jnp.bfloat16)


def up_project(part, col, parts, weight, slots):
    tp = len(parts)
    rows, width = parts[0].shape
    depth, units = weight.shape
    block = min(256, units)
    grid_spec = pltpu.PrefetchScalarGridSpec(
        num_scalar_prefetch=2,
        grid=(units // block,),
        in_specs=[pl.BlockSpec((rows, width), lambda n, a, b: (0, 0))] * tp
        + [pl.BlockSpec((depth, block), lambda n, a, b: (0, n))],
        out_specs=pl.BlockSpec((rows, block), lambda n, a, b: (0, n)),
        scratch_shapes=[pltpu.VMEM((rows, depth), jnp.bfloat16)],
    )
    return pl.pallas_call(
        functools.partial(up_kernel, tp=tp, slots=slots, slab=depth // slots),
        grid_spec=grid_spec,
        out_shape=jax.ShapeDtypeStruct((rows, units), jnp.bfloat16),
        cost_estimate=pl.CostEstimate(
            flops=2 * rows * depth * units, bytes_accessed=2 * depth * (units + rows), transcendentals=0
        ),
    )(part, col, *parts, weight)


def down_kernel(part, col, x_ref, w_ref, *out_refs, slab):
    s = pl.program_id(0)
    result = jnp.dot(x_ref[...], w_ref[...], preferred_element_type=jnp.float32).astype(jnp.bfloat16)
    for j, out_ref in enumerate(out_refs):

        @pl.when(part[s] == j)
        def _(out_ref=out_ref):
            out_ref[:, pl.ds(pl.multiple_of(col[s], slab), slab)] = result


def down_project(part, col, squared, weight, tp, slots):
    rows, units = squared.shape
    slab = weight.shape[1]
    width = slab * slots // tp
    grid_spec = pltpu.PrefetchScalarGridSpec(
        num_scalar_prefetch=2,
        grid=(slots,),
        in_specs=[
            pl.BlockSpec((rows, units), lambda s, a, b: (0, 0)),
            pl.BlockSpec((units, slab), lambda s, a, b: (s, 0)),
        ],
        out_specs=[pl.BlockSpec((rows, width), lambda s, a, b: (0, 0))] * tp,
    )
    return pl.pallas_call(
        functools.partial(down_kernel, slab=slab),
        grid_spec=grid_spec,
        out_shape=[jax.ShapeDtypeStruct((rows, width), jnp.bfloat16)] * tp,
        cost_estimate=pl.CostEstimate(
            flops=2 * rows * units * slab * slots, bytes_accessed=2 * units * (slab * slots + rows), transcendentals=0
        ),
    )(part, col, squared, weight)


def make_body(outer, inner, tp):
    def swap_outer(value, k):
        pairs = [(o * inner + i, (o ^ k) * inner + i) for o in range(outer) for i in range(inner)]
        return lax.ppermute(value, "sp", pairs)

    def swap_inner(value, r):
        pairs = [(o * inner + i, o * inner + (i ^ r)) for o in range(outer) for i in range(inner)]
        return lax.ppermute(value, "sp", pairs)

    def swap_tp(value, j):
        return lax.ppermute(value, "tp", [(t, t ^ j) for t in range(tp)])

    def gather_inner(value):
        if inner != 4:
            return [value] + [swap_inner(value, r) for r in range(1, inner)]
        half = value.shape[0] // 2
        first, second = swap_inner(value, 1), swap_inner(value, 2)
        corner_a = swap_inner(second[:half], 1)
        corner_b = swap_inner(first[half:], 2)
        return [value, first, second, corner_a, corner_b]

    def body(
        queries, keys, values, documents, query_gain, key_gain, residual, out_weight, norm_gain, up_weight, down_weight
    ):
        rows = queries.shape[0]
        key_heads = keys.shape[1] // HD
        group = HQ // KV
        width = residual.shape[1]
        sp_index = lax.axis_index("sp")
        o, i, t = sp_index // inner, sp_index % inner, lax.axis_index("tp")
        split = key_heads % outer == 0
        units = up_weight.shape[1] // outer
        slab = up_weight.shape[0]
        far = range(1, outer)
        places = [(r, k) for r in range(inner) for k in (0,)] + [(r, k) for r in range(inner) for k in far]
        slots = len(places)
        spots = jnp.stack([((o ^ k) * inner + (i ^ r)) * slab for r, k in places]).astype(jnp.int32)
        part = (spots // width) ^ t.astype(jnp.int32)
        col = spots % width

        docs_outer = jnp.stack([documents] + [swap_outer(documents, k) for k in far])
        docs_all = jnp.concatenate([docs_outer] + [swap_inner(docs_outer, r) for r in range(1, inner)])

        up_near = gather_inner(lax.dynamic_slice_in_dim(up_weight, o * units, units, 1))
        down_near = gather_inner(lax.dynamic_slice_in_dim(down_weight, o * units, units, 0))
        up_pieces = [swap_outer(lax.dynamic_slice_in_dim(up_weight, (o ^ k) * units, units, 1), k) for k in far]
        down_pieces = [swap_outer(lax.dynamic_slice_in_dim(down_weight, (o ^ k) * units, units, 0), k) for k in far]
        up_far = gather_inner(jnp.concatenate(up_pieces))
        down_far = gather_inner(jnp.concatenate(down_pieces))

        positions = sp_index * rows + jnp.arange(rows, dtype=jnp.int32)
        queries_rot = grid_rotary(
            head_norm(queries.reshape(rows, key_heads * group, HD), query_gain), positions
        ).astype(jnp.bfloat16)
        keys_rot = grid_rotary(head_norm(keys.reshape(rows, key_heads, HD), key_gain), positions).astype(jnp.bfloat16)
        parts = outer if split else 1
        heads = key_heads // parts
        q_width = heads * group * HD
        packed = jnp.concatenate(
            [
                queries_rot.reshape(rows, parts, q_width),
                keys_rot.reshape(rows, parts, heads * HD),
                values.reshape(rows, parts, heads * HD),
            ],
            axis=-1,
        )
        packed = jnp.transpose(packed, (1, 0, 2))
        if split:
            taken = [lax.dynamic_index_in_dim(packed, o ^ k, 0, keepdims=False) for k in range(outer)]
            taken = [taken[0]] + [swap_outer(taken[k], k) for k in far]
            q_blocks = jnp.stack([piece[:, :q_width] for piece in taken])
            kv_own = jnp.concatenate([piece[:, q_width:] for piece in taken])
            q_docs = docs_outer
        else:
            q_blocks = packed[:, :, :q_width]
            kv_mine = packed[0, :, q_width:]
            kv_own = jnp.concatenate([kv_mine] + [swap_outer(kv_mine, k) for k in far])
            q_docs = documents[None]
        kv_all = jnp.concatenate(gather_inner(kv_own)).reshape(outer * inner, rows, -1)

        attended = []
        for h in range(heads):
            q_head = q_blocks[:, :, h * group * HD : (h + 1) * group * HD]
            kv_head = kv_all
            if heads > 1:
                kv_head = jnp.concatenate(
                    [kv_all[:, :, h * HD : (h + 1) * HD], kv_all[:, :, (heads + h) * HD : (heads + h + 1) * HD]], -1
                )
            attended.append(attend(q_head, kv_head, q_docs, docs_all, group))
        attended = attended[0] if heads == 1 else jnp.concatenate(attended, -1)
        if split:
            merged = jnp.zeros((rows, outer * q_width), jnp.bfloat16)
            for k in range(outer):
                piece = attended[k] if k == 0 else swap_outer(attended[k], k)
                merged = lax.dynamic_update_slice_in_dim(merged, piece, (o ^ k) * q_width, 1)
            attended = merged
        else:
            attended = attended[0]

        partial_out = jnp.dot(attended, out_weight, preferred_element_type=jnp.float32).astype(jnp.bfloat16)
        stream = residual.astype(jnp.float32)
        for j in range(tp):
            piece = lax.dynamic_slice_in_dim(partial_out, (t ^ j) * width, width, 1)
            piece = piece if j == 0 else swap_tp(piece, j)
            stream = stream + piece.astype(jnp.float32)
        squares = jnp.sum(stream * stream, axis=-1)
        total_squares = squares
        for j in range(1, tp):
            total_squares = total_squares + swap_tp(squares, j)
        gain_here = lax.dynamic_slice_in_dim(norm_gain, t * width, width, 0)
        normed = stream * lax.rsqrt(total_squares / (width * tp) + norm_eps)[:, None]
        normed = (normed * gain_here).astype(jnp.bfloat16)

        up_whole = jnp.concatenate(up_near + up_far)
        down_whole = jnp.concatenate(down_near + down_far)

        squared = []
        for k in range(outer):
            chunk = normed if k == 0 else swap_outer(normed, k)
            chunk_parts = [chunk]
            for j in range(1, tp):
                chunk_parts.append(swap_tp(chunk, j))
            squared.append(up_project(part, col, chunk_parts, up_whole, slots))
        feed = [None] * outer
        for k in list(far)[::-1] + [0]:
            pieces = down_project(part, col, squared[k], down_whole, tp, slots)
            total = pieces[0].astype(jnp.float32)
            for j in range(1, tp):
                total = total + swap_tp(pieces[j], j).astype(jnp.float32)
            feed[k] = total if k == 0 else swap_outer(total.astype(jnp.bfloat16), k)
        result = stream
        for k in range(outer):
            result = result + feed[k].astype(jnp.float32)
        return result.astype(jnp.bfloat16)

    return body


def solution(mesh):
    sp, tp = mesh.shape["sp"], mesh.shape["tp"]
    outer = 1 << (sp.bit_length() // 2)
    inner = sp // outer
    in_specs = (
        P("sp", "tp"),
        P("sp", "tp"),
        P("sp", "tp"),
        P("sp"),
        P(),
        P(),
        P("sp", "tp"),
        P("tp", None),
        P(),
        P("sp", "tp"),
        P("tp", "sp"),
    )
    return jax.shard_map(
        make_body(outer, inner, tp), mesh=mesh, in_specs=in_specs, out_specs=P("sp", "tp"), check_vma=False
    )
```

time: 2440 us -> 967 us (0.40)
  the two profiles are of different devices: /device:TPU:0 before, /device:TPU:10 now
where the time goes in v1:
time: 967 us; the launch traced here: 956 us
  waiting for transfers between devices  573 us (59%)
  Pallas kernels  194 us (20%)
  local copies, waits for them, and re-layouts  91.3 us (9%)
  starting transfers between devices  57.6 us (6%)
  other arithmetic  31.4 us (3%)
    ppermute x21, waiting for transfers between devices, swap_outer(): return lax.ppermute(value, 'sp', pairs)  384 us
    ppermute x23, waiting for transfers between devices, swap_inner(): return lax.ppermute(value, 'sp', pairs)  188 us
    pallas_call x4, Pallas kernels, down_project(): pl.pallas_call(functools.partial(down_kernel, slab=slab), grid_spec=grid_...  82.1 us
    pallas_call x4, Pallas kernels, up_project(): pl.pallas_call(functools.partial(up_kernel, tp=tp, slots=slots, slab=dept...  67.3 us
    pallas_call x1, Pallas kernels, attend(): pl.pallas_call(functools.partial(attend_kernel, group=group, blocks=block...  44.2 us
    unnamed x59, local copies, waits for them, and re-layouts  43.7 us
    ppermute x23, starting transfers between devices, swap_inner(): return lax.ppermute(value, 'sp', pairs)  30.4 us
    ppermute x21, starting transfers between devices, swap_outer(): return lax.ppermute(value, 'sp', pairs)  26 us
  transfers between devices with their start and end apart: 54, of which 21 were waited for; matrix products, arithmetic and copies ran while one was open for 13% of the time, Pallas kernels for 20%

profile of v1, /device:TPU:10, one launch (start us, length us, event | category | flops | bytes accessed | tf_op | source)
XLA Modules:
  0.0 956.1 jit_solution(5805483264478256364)
XLA Ops:
  18.9 4.8 constant_dynamic-slice_fusion
  39.4 14.6 %collective-permute-done.7 = bf16[512,512]{1,0:T(8,128)(2,1)} collective-permute-done((bf16[512,512]{1,0:T(8,128)(2,1)}, bf16[512,512]{1,0:T(8,128)(2,1)}, u32[]{:S(2)}, u32[]{:S(2)}) %collective-permute-start.7) | collective-permute-done | bytes 524320 | tf_op jit(solution)/shard_map/ppermute | solution.py:225
  57.4 6.8 collective-permute-done.8
  75.0 6.6 collective-permute-done.19
  87.2 17.3 %collective-permute-done.10 = bf16[2048,256]{1,0:T(8,128)(2,1)S(1)} collective-permute-done((bf16[2048,256]{1,0:T(8,128)(2,1)}, bf16[2048,256]{1,0:T(8,128)(2,1)S(1)}, u32[]{:S(2)}, u32[]{:S(2)}) %collective-permute-start.10) | collective-permute-done | bytes 1048608 | tf_op jit(solution)/shard_map/ppermute | solution.py:229
  123.7 44.3 %collective-permute-done.35 = bf16[2048,256]{1,0:T(8,128)(2,1)S(1)} collective-permute-done((bf16[2048,256]{1,0:T(8,128)(2,1)S(1)}, bf16[2048,256]{1,0:T(8,128)(2,1)S(1)}, u32[]{:S(2)}, u32[]{:S(2)}) %collective-permute-start.35) | collective-permute-done | bytes 1048608 | tf_op jit(solution)/shard_map/ppermute | solution.py:225
  175.2 44.2 %attend.1 = bf16[2048,256]{1,0:T(8,128)(2,1)} custom-call(s32[128]{0:T(128)} %select_n.108.flags, bf16[2048,256]{1,0:T(8,128)(2,1)} %bitcast.54, bf16[16,512,256]{2,1,0:T(8,128)(2,1)} %bitcast.57, s32[8,1,512]{2,1,0:T(1,128)} %tile.8.qdoc_ref, s32[16,512,1]{2,1,0:T(8,128)} %copy.83.kdoc_ref), custom_call_target="tpu_custom_call" | custom-call | flops 8589934592 | bytes 6291456 | tf_op jit(solution)/shard_map/attend/pallas_call | solution.py:136
  226.8 8.7 collective-permute-done.13
  235.6 39.2 %collective-permute-done.14 = bf16[512,256]{1,0:T(8,128)(2,1)S(1)} collective-permute-done((bf16[512,256]{1,0:T(8,128)(2,1)S(1)}, bf16[512,256]{1,0:T(8,128)(2,1)S(1)}, u32[]{:S(2)}, u32[]{:S(2)}) %collective-permute-start.14) | collective-permute-done | bytes 262176 | tf_op jit(solution)/shard_map/ppermute | solution.py:225
  276.3 5.3 collective-permute-done.15
  283.1 8.6 convolution_convert_fusion
  313.9 4.5 multiply_convert_fusion.refs_0_
  318.3 34.5 %collective-permute-done.38 = bf16[6144,256]{1,0:T(8,128)(2,1)} collective-permute-done((bf16[6144,256]{1,0:T(8,128)(2,1)}, bf16[6144,256]{1,0:T(8,128)(2,1)}, u32[]{:S(2)}, u32[]{:S(2)}) %collective-permute-start.38) | collective-permute-done | bytes 3145760 | tf_op jit(solution)/shard_map/ppermute | solution.py:229
  359.2 60.5 %collective-permute-done.27 = bf16[768,2048]{1,0:T(8,128)(2,1)} collective-permute-done((bf16[768,2048]{1,0:T(8,128)(2,1)}, bf16[768,2048]{1,0:T(8,128)(2,1)}, u32[]{:S(2)}, u32[]{:S(2)}) %collective-permute-start.27) | collective-permute-done | bytes 3145760 | tf_op jit(solution)/shard_map/ppermute | solution.py:229
  431.7 14.2 %collective-permute-done.26 = bf16[768,2048]{1,0:T(8,128)(2,1)} collective-permute-done((bf16[768,2048]{1,0:T(8,128)(2,1)}, bf16[768,2048]{1,0:T(8,128)(2,1)}, u32[]{:S(2)}, u32[]{:S(2)}) %collective-permute-start.26) | collective-permute-done | bytes 3145760 | tf_op jit(solution)/shard_map/ppermute | solution.py:229
  451.5 28.1 %collective-permute-done.39 = bf16[3072,256]{1,0:T(8,128)(2,1)} collective-permute-done((bf16[3072,256]{1,0:T(8,128)(2,1)}, bf16[3072,256]{1,0:T(8,128)(2,1)}, u32[]{:S(2)}, u32[]{:S(2)}) %collective-permute-start.39) | collective-permute-done | bytes 1572896 | tf_op jit(solution)/shard_map/ppermute | solution.py:229
  480.1 4.0 constant_dynamic-update-slice_fusion.14
  485.7 26.4 %collective-permute-done.28 = bf16[384,2048]{1,0:T(8,128)(2,1)S(1)} collective-permute-done((bf16[384,2048]{1,0:T(8,128)(2,1)S(1)}, bf16[384,2048]{1,0:T(8,128)(2,1)S(1)}, u32[]{:S(2)}, u32[]{:S(2)}) %collective-permute-start.28) | collective-permute-done | bytes 1572896 | tf_op jit(solution)/shard_map/ppermute | solution.py:229
  520.4 43.2 %collective-permute-done.46.refs_0_ = bf16[512,2048]{1,0:T(8,128)(2,1)} collective-permute-done((bf16[512,2048]{1,0:T(8,128)(2,1)}, bf16[512,2048]{1,0:T(8,128)(2,1)}, u32[]{:S(2)}, u32[]{:S(2)}) %collective-permute-start.46) | collective-permute-done | bytes 2097184 | tf_op jit(solution)/shard_map/ppermute | solution.py:225
  566.2 40.1 %collective-permute-done.50.refs_0_ = bf16[512,2048]{1,0:T(8,128)(2,1)} collective-permute-done((bf16[512,2048]{1,0:T(8,128)(2,1)}, bf16[512,2048]{1,0:T(8,128)(2,1)}, u32[]{:S(2)}, u32[]{:S(2)}) %collective-permute-start.50) | collective-permute-done | bytes 2097184 | tf_op jit(solution)/shard_map/ppermute | solution.py:225
  606.3 16.8 %shard_map.111.x_ref = bf16[512,2048]{1,0:T(8,128)(2,1)} custom-call(s32[16]{0:T(128)} %get-tuple-element.84.part, s32[16]{0:T(128)} %get-tuple-element.83.col, bf16[512,2048]{1,0:T(8,128)(2,1)} %collective-permute-done.42.refs_0_, bf16[512,2048]{1,0:T(8,128)(2,1)} %collective-permute-done.43.refs_1_, ...), custom_call_target="tpu_custom_call" | custom-call | flops 8589934592 | bytes 20971520 | tf_op jit(solution)/shard_map/pallas_call | solution.py:179
  623.1 20.5 %shard_map.112 = (bf16[512,2048]{1,0:T(8,128)(2,1)}, bf16[512,2048]{1,0:T(8,128)(2,1)}) custom-call(s32[16]{0:T(128)} %get-tuple-element.84.part, s32[16]{0:T(128)} %get-tuple-element.83.col, bf16[512,2048]{1,0:T(8,128)(2,1)} %shard_map.111.x_ref, bf16[32768,256]{1,0:T(8,128)(2,1)} %constant_dynamic-update-slice_fusion.27.w_ref), custom_call_target="tpu_custom_call" | custom-call | flops 8589934592 | bytes 18874368 | tf_op jit(solution)/shard_map/pallas_call | solution.py:212
  644.1 17.0 %shard_map.113.x_ref = bf16[512,2048]{1,0:T(8,128)(2,1)} custom-call(s32[16]{0:T(128)} %get-tuple-element.84.part, s32[16]{0:T(128)} %get-tuple-element.83.col, bf16[512,2048]{1,0:T(8,128)(2,1)} %collective-permute-done.46.refs_0_, bf16[512,2048]{1,0:T(8,128)(2,1)} %collective-permute-done.47.refs_1_, ...), custom_call_target="tpu_custom_call" | custom-call | flops 8589934592 | bytes 20971520 | tf_op jit(solution)/shard_map/pallas_call | solution.py:179
  661.0 20.5 %shard_map.114 = (bf16[512,2048]{1,0:T(8,128)(2,1)}, bf16[512,2048]{1,0:T(8,128)(2,1)}) custom-call(s32[16]{0:T(128)} %get-tuple-element.84.part, s32[16]{0:T(128)} %get-tuple-element.83.col, bf16[512,2048]{1,0:T(8,128)(2,1)} %shard_map.113.x_ref, bf16[32768,256]{1,0:T(8,128)(2,1)} %constant_dynamic-update-slice_fusion.27.w_ref), custom_call_target="tpu_custom_call" | custom-call | flops 8589934592 | bytes 18874368 | tf_op jit(solution)/shard_map/pallas_call | solution.py:212
  681.5 16.8 %shard_map.115.x_ref = bf16[512,2048]{1,0:T(8,128)(2,1)} custom-call(s32[16]{0:T(128)} %get-tuple-element.84.part, s32[16]{0:T(128)} %get-tuple-element.83.col, bf16[512,2048]{1,0:T(8,128)(2,1)} %collective-permute-done.50.refs_0_, bf16[512,2048]{1,0:T(8,128)(2,1)} %collective-permute-done.51.refs_1_, ...), custom_call_target="tpu_custom_call" | custom-call | flops 8589934592 | bytes 20971520 | tf_op jit(solution)/shard_map/pallas_call | solution.py:179
  698.3 20.4 %shard_map.116 = (bf16[512,2048]{1,0:T(8,128)(2,1)}, bf16[512,2048]{1,0:T(8,128)(2,1)}) custom-call(s32[16]{0:T(128)} %get-tuple-element.84.part, s32[16]{0:T(128)} %get-tuple-element.83.col, bf16[512,2048]{1,0:T(8,128)(2,1)} %shard_map.115.x_ref, bf16[32768,256]{1,0:T(8,128)(2,1)} %constant_dynamic-update-slice_fusion.27.w_ref), custom_call_target="tpu_custom_call" | custom-call | flops 8589934592 | bytes 18874368 | tf_op jit(solution)/shard_map/pallas_call | solution.py:212
  719.2 16.8 %shard_map.109.x_ref = bf16[512,2048]{1,0:T(8,128)(2,1)} custom-call(s32[16]{0:T(128)} %get-tuple-element.84.part, s32[16]{0:T(128)} %get-tuple-element.83.col, bf16[512,2048]{1,0:T(8,128)(2,1)} %multiply_convert_fusion.refs_0_, bf16[512,2048]{1,0:T(8,128)(2,1)} %collective-permute-done.18.refs_1_, ...), custom_call_target="tpu_custom_call" | custom-call | flops 8589934592 | bytes 20971520 | tf_op jit(solution)/shard_map/pallas_call | solution.py:179
  736.0 20.7 %shard_map.110 = (bf16[512,2048]{1,0:T(8,128)(2,1)}, bf16[512,2048]{1,0:T(8,128)(2,1)}) custom-call(s32[16]{0:T(128)} %get-tuple-element.84.part, s32[16]{0:T(128)} %get-tuple-element.83.col, bf16[512,2048]{1,0:T(8,128)(2,1)} %shard_map.109.x_ref, bf16[32768,256]{1,0:T(8,128)(2,1)} %constant_dynamic-update-slice_fusion.27.w_ref), custom_call_target="tpu_custom_call" | custom-call | flops 8589934592 | bytes 18874368 | tf_op jit(solution)/shard_map/pallas_call | solution.py:212
  768.5 79.3 %collective-permute-done.45 = bf16[512,2048]{1,0:T(8,128)(2,1)S(1)} collective-permute-done((bf16[512,2048]{1,0:T(8,128)(2,1)S(1)}, bf16[512,2048]{1,0:T(8,128)(2,1)S(1)}, u32[]{:S(2)}, u32[]{:S(2)}) %collective-permute-start.45) | collective-permute-done | bytes 2097184 | tf_op jit(solution)/shard_map/ppermute | solution.py:225
  847.8 53.3 %collective-permute-done.49 = bf16[512,2048]{1,0:T(8,128)(2,1)S(1)} collective-permute-done((bf16[512,2048]{1,0:T(8,128)(2,1)S(1)}, bf16[512,2048]{1,0:T(8,128)(2,1)S(1)}, u32[]{:S(2)}, u32[]{:S(2)}) %collective-permute-start.49) | collective-permute-done | bytes 2097184 | tf_op jit(solution)/shard_map/ppermute | solution.py:225
  901.1 45.5 %collective-permute-done.53 = bf16[512,2048]{1,0:T(8,128)(2,1)S(1)} collective-permute-done((bf16[512,2048]{1,0:T(8,128)(2,1)S(1)}, bf16[512,2048]{1,0:T(8,128)(2,1)S(1)}, u32[]{:S(2)}, u32[]{:S(2)}) %collective-permute-start.53) | collective-permute-done | bytes 2097184 | tf_op jit(solution)/shard_map/ppermute | solution.py:225
  946.6 9.3 add_convert_fusion
  (220 shorter events, 162.6 us)
Async XLA Ops:
  35.9 45.7 %collective-permute-start.19 = (bf16[256,2048]{1,0:T(8,128)(2,1)}, bf16[256,2048]{1,0:T(8,128)(2,1)}, u32[]{:S(2)}, u32[]{:S(2)}) collective-permute-start(bf16[256,2048]{1,0:T(8,128)(2,1)} %get-tuple-element.35), channel_id=1, source_target_pairs={{0,2},{2,0},{4,6},{6,4},{8,10},{10,8},{12,14},{14,12},{16,18},{18,... | collective-permute-start | bytes 3145736 | tf_op jit(solution)/shard_map/ppermute | solution.py:229
  73.9 45.7 %collective-permute-start.34 = (bf16[2048,256]{1,0:T(8,128)(2,1)}, bf16[2048,256]{1,0:T(8,128)(2,1)S(1)}, u32[]{:S(2)}, u32[]{:S(2)}) collective-permute-start(bf16[2048,256]{1,0:T(8,128)(2,1)} %get-tuple-element.28), channel_id=1, source_target_pairs={{0,8},{2,10},{4,12},{6,14},{8,0},{10,2},{12,4},{14,6},{16,24},{18,... | collective-permute-start | bytes 3145736 | tf_op jit(solution)/shard_map/ppermute | solution.py:225
  104.5 63.5 %collective-permute-start.35 = (bf16[2048,256]{1,0:T(8,128)(2,1)S(1)}, bf16[2048,256]{1,0:T(8,128)(2,1)S(1)}, u32[]{:S(2)}, u32[]{:S(2)}) collective-permute-start(bf16[2048,256]{1,0:T(8,128)(2,1)S(1)} %copy-done.12), channel_id=1, source_target_pairs={{0,16},{2,18},{4,20},{6,22},{8,24},{10,26},{12,28},{14,30},{16,0},... | collective-permute-start | bytes 3145736 | tf_op jit(solution)/shard_map/ppermute | solution.py:225
  112.3 108.7 %collective-permute-start.36 = (bf16[2048,256]{1,0:T(8,128)(2,1)}, bf16[2048,256]{1,0:T(8,128)(2,1)S(1)}, u32[]{:S(2)}, u32[]{:S(2)}) collective-permute-start(bf16[2048,256]{1,0:T(8,128)(2,1)} %get-tuple-element.27), channel_id=1, source_target_pairs={{0,24},{2,26},{4,28},{6,30},{8,16},{10,18},{12,20},{14,22},{16,8},... | collective-permute-start | bytes 3145736 | tf_op jit(solution)/shard_map/ppermute | solution.py:225
  113.3 181.3 %collective-permute-start.23 = (bf16[256,2048]{1,0:T(8,128)(2,1)}, bf16[256,2048]{1,0:T(8,128)(2,1)}, u32[]{:S(2)}, u32[]{:S(2)}) collective-permute-start(bf16[256,2048]{1,0:T(8,128)(2,1)} %get-tuple-element.33), channel_id=1, source_target_pairs={{0,8},{2,10},{4,12},{6,14},{8,0},{10,2},{12,4},{14,6},{16,24},{18,... | collective-permute-start | bytes 3145736 | tf_op jit(solution)/shard_map/ppermute | solution.py:225
  116.1 56.7 %collective-permute-start.11 = (bf16[1024,256]{1,0:T(8,128)(2,1)S(1)}, bf16[1024,256]{1,0:T(8,128)(2,1)S(1)}, u32[]{:S(2)}, u32[]{:S(2)}) collective-permute-start(bf16[1024,256]{1,0:T(8,128)(2,1)S(1)} %slice.172), channel_id=1, source_target_pairs={{0,2},{2,0},{4,6},{6,4},{8,10},{10,8},{12,14},{14,12},{16,18},{18,... | collective-permute-start | bytes 1572872 | tf_op jit(solution)/shard_map/ppermute | solution.py:229
  119.5 54.8 %collective-permute-start.12 = (bf16[1024,256]{1,0:T(8,128)(2,1)S(1)}, bf16[1024,256]{1,0:T(8,128)(2,1)S(1)}, u32[]{:S(2)}, u32[]{:S(2)}) collective-permute-start(bf16[1024,256]{1,0:T(8,128)(2,1)S(1)} %slice.173), channel_id=1, source_target_pairs={{0,4},{2,6},{4,0},{6,2},{8,12},{10,14},{12,8},{14,10},{16,20},{18,... | collective-permute-start | bytes 1572872 | tf_op jit(solution)/shard_map/ppermute | solution.py:229
  168.0 129.6 %collective-permute-start.24 = (bf16[256,2048]{1,0:T(8,128)(2,1)S(1)}, bf16[256,2048]{1,0:T(8,128)(2,1)}, u32[]{:S(2)}, u32[]{:S(2)}) collective-permute-start(bf16[256,2048]{1,0:T(8,128)(2,1)S(1)} %copy-done.11), channel_id=1, source_target_pairs={{0,16},{2,18},{4,20},{6,22},{8,24},{10,26},{12,28},{14,30},{16,0},... | collective-permute-start | bytes 3145736 | tf_op jit(solution)/shard_map/ppermute | solution.py:225
  172.8 52.6 %collective-permute-start.21 = (bf16[128,2048]{1,0:T(8,128)(2,1)}, bf16[128,2048]{1,0:T(8,128)(2,1)S(1)}, u32[]{:S(2)}, u32[]{:S(2)}) collective-permute-start(bf16[128,2048]{1,0:T(8,128)(2,1)} %slice.178), channel_id=1, source_target_pairs={{0,2},{2,0},{4,6},{6,4},{8,10},{10,8},{12,14},{14,12},{16,18},{18,... | collective-permute-start | bytes 1572872 | tf_op jit(solution)/shard_map/ppermute | solution.py:229
  222.5 52.2 %collective-permute-start.14 = (bf16[512,256]{1,0:T(8,128)(2,1)S(1)}, bf16[512,256]{1,0:T(8,128)(2,1)S(1)}, u32[]{:S(2)}, u32[]{:S(2)}) collective-permute-start(bf16[512,256]{1,0:T(8,128)(2,1)S(1)} %get-tuple-element.60), channel_id=1, source_target_pairs={{0,16},{2,18},{4,20},{6,22},{8,24},{10,26},{12,28},{14,30},{16,0},... | collective-permute-start | bytes 786440 | tf_op jit(solution)/shard_map/ppermute | solution.py:225
  225.5 56.1 %collective-permute-start.15 = (bf16[512,256]{1,0:T(8,128)(2,1)S(1)}, bf16[512,256]{1,0:T(8,128)(2,1)S(1)}, u32[]{:S(2)}, u32[]{:S(2)}) collective-permute-start(bf16[512,256]{1,0:T(8,128)(2,1)S(1)} %get-tuple-element.59), channel_id=1, source_target_pairs={{0,24},{2,26},{4,28},{6,30},{8,16},{10,18},{12,20},{14,22},{16,8},... | collective-permute-start | bytes 786440 | tf_op jit(solution)/shard_map/ppermute | solution.py:225
  235.5 68.4 %collective-permute-start.25 = (bf16[256,2048]{1,0:T(8,128)(2,1)S(1)}, bf16[256,2048]{1,0:T(8,128)(2,1)S(1)}, u32[]{:S(2)}, u32[]{:S(2)}) collective-permute-start(bf16[256,2048]{1,0:T(8,128)(2,1)S(1)} %copy-done.10), channel_id=1, source_target_pairs={{0,24},{2,26},{4,28},{6,30},{8,16},{10,18},{12,20},{14,22},{16,8},... | collective-permute-start | bytes 3145736 | tf_op jit(solution)/shard_map/ppermute | solution.py:225
  281.6 71.3 %collective-permute-start.38 = (bf16[6144,256]{1,0:T(8,128)(2,1)}, bf16[6144,256]{1,0:T(8,128)(2,1)}, u32[]{:S(2)}, u32[]{:S(2)}) collective-permute-start(bf16[6144,256]{1,0:T(8,128)(2,1)} %get-tuple-element.47), channel_id=1, source_target_pairs={{0,4},{2,6},{4,0},{6,2},{8,12},{10,14},{12,8},{14,10},{16,20},{18,... | collective-permute-start | bytes 9437192 | tf_op jit(solution)/shard_map/ppermute | solution.py:229
  305.7 114.0 %collective-permute-start.27 = (bf16[768,2048]{1,0:T(8,128)(2,1)}, bf16[768,2048]{1,0:T(8,128)(2,1)}, u32[]{:S(2)}, u32[]{:S(2)}) collective-permute-start(bf16[768,2048]{1,0:T(8,128)(2,1)} %get-tuple-element.53), channel_id=1, source_target_pairs={{0,4},{2,6},{4,0},{6,2},{8,12},{10,14},{12,8},{14,10},{16,20},{18,... | collective-permute-start | bytes 9437192 | tf_op jit(solution)/shard_map/ppermute | solution.py:229
  307.2 117.3 %collective-permute-start.37 = (bf16[6144,256]{1,0:T(8,128)(2,1)}, bf16[6144,256]{1,0:T(8,128)(2,1)}, u32[]{:S(2)}, u32[]{:S(2)}) collective-permute-start(bf16[6144,256]{1,0:T(8,128)(2,1)} %get-tuple-element.47), channel_id=1, source_target_pairs={{0,2},{2,0},{4,6},{6,4},{8,10},{10,8},{12,14},{14,12},{16,18},{18,... | collective-permute-start | bytes 9437192 | tf_op jit(solution)/shard_map/ppermute | solution.py:229
  308.6 137.3 %collective-permute-start.26 = (bf16[768,2048]{1,0:T(8,128)(2,1)}, bf16[768,2048]{1,0:T(8,128)(2,1)}, u32[]{:S(2)}, u32[]{:S(2)}) collective-permute-start(bf16[768,2048]{1,0:T(8,128)(2,1)} %get-tuple-element.53), channel_id=1, source_target_pairs={{0,2},{2,0},{4,6},{6,4},{8,10},{10,8},{12,14},{14,12},{16,18},{18,... | collective-permute-start | bytes 9437192 | tf_op jit(solution)/shard_map/ppermute | solution.py:229
  318.3 161.8 %collective-permute-start.42 = (bf16[512,2048]{1,0:T(8,128)(2,1)}, bf16[512,2048]{1,0:T(8,128)(2,1)}, u32[]{:S(2)}, u32[]{:S(2)}) collective-permute-start(bf16[512,2048]{1,0:T(8,128)(2,1)} %multiply_convert_fusion.refs_0_), channel_id=1, source_target_pairs={{0,8},{2,10},{4,12},{6,14},{8,0},{10,2},{12,4},{14,6},{16,24},{18,... | collective-permute-start | bytes 6291464 | tf_op jit(solution)/shard_map/ppermute | solution.py:225
  355.5 124.1 %collective-permute-start.39 = (bf16[3072,256]{1,0:T(8,128)(2,1)}, bf16[3072,256]{1,0:T(8,128)(2,1)}, u32[]{:S(2)}, u32[]{:S(2)}) collective-permute-start(bf16[3072,256]{1,0:T(8,128)(2,1)} %slice.184), channel_id=1, source_target_pairs={{0,2},{2,0},{4,6},{6,4},{8,10},{10,8},{12,14},{14,12},{16,18},{18,... | collective-permute-start | bytes 4718600 | tf_op jit(solution)/shard_map/ppermute | solution.py:229
  421.2 90.9 %collective-permute-start.28 = (bf16[384,2048]{1,0:T(8,128)(2,1)S(1)}, bf16[384,2048]{1,0:T(8,128)(2,1)S(1)}, u32[]{:S(2)}, u32[]{:S(2)}) collective-permute-start(bf16[384,2048]{1,0:T(8,128)(2,1)S(1)} %slice.180), channel_id=1, source_target_pairs={{0,2},{2,0},{4,6},{6,4},{8,10},{10,8},{12,14},{14,12},{16,18},{18,... | collective-permute-start | bytes 4718600 | tf_op jit(solution)/shard_map/ppermute | solution.py:229
  424.5 139.1 %collective-permute-start.46 = (bf16[512,2048]{1,0:T(8,128)(2,1)}, bf16[512,2048]{1,0:T(8,128)(2,1)}, u32[]{:S(2)}, u32[]{:S(2)}) collective-permute-start(bf16[512,2048]{1,0:T(8,128)(2,1)} %multiply_convert_fusion.refs_0_), channel_id=1, source_target_pairs={{0,16},{2,18},{4,20},{6,22},{8,24},{10,26},{12,28},{14,30},{16,0},... | collective-permute-start | bytes 6291464 | tf_op jit(solution)/shard_map/ppermute | solution.py:225
  445.9 160.4 %collective-permute-start.50 = (bf16[512,2048]{1,0:T(8,128)(2,1)}, bf16[512,2048]{1,0:T(8,128)(2,1)}, u32[]{:S(2)}, u32[]{:S(2)}) collective-permute-start(bf16[512,2048]{1,0:T(8,128)(2,1)} %multiply_convert_fusion.refs_0_), channel_id=1, source_target_pairs={{0,24},{2,26},{4,28},{6,30},{8,16},{10,18},{12,20},{14,22},{16,8},... | collective-permute-start | bytes 6291464 | tf_op jit(solution)/shard_map/ppermute | solution.py:225
  480.1 126.2 %collective-permute-start.43 = (bf16[512,2048]{1,0:T(8,128)(2,1)}, bf16[512,2048]{1,0:T(8,128)(2,1)}, u32[]{:S(2)}, u32[]{:S(2)}) collective-permute-start(bf16[512,2048]{1,0:T(8,128)(2,1)} %collective-permute-done.42.refs_0_), channel_id=1, source_target_pairs={{0,1},{1,0},{2,3},{3,2},{4,5},{5,4},{6,7},{7,6},{8,9},{9,8},{10,11... | collective-permute-start | bytes 6291464 | tf_op jit(solution)/shard_map/ppermute | solution.py:232
  512.1 52.9 %collective-permute-start.40 = (bf16[3072,256]{1,0:T(8,128)(2,1)S(1)}, bf16[3072,256]{1,0:T(8,128)(2,1)S(1)}, u32[]{:S(2)}, u32[]{:S(2)}) collective-permute-start(bf16[3072,256]{1,0:T(8,128)(2,1)S(1)} %slice.185), channel_id=1, source_target_pairs={{0,4},{2,6},{4,0},{6,2},{8,12},{10,14},{12,8},{14,10},{16,20},{18,... | collective-permute-start | bytes 4718600 | tf_op jit(solution)/shard_map/ppermute | solution.py:229
  520.4 198.8 %collective-permute-start.18 = (bf16[512,2048]{1,0:T(8,128)(2,1)}, bf16[512,2048]{1,0:T(8,128)(2,1)}, u32[]{:S(2)}, u32[]{:S(2)}) collective-permute-start(bf16[512,2048]{1,0:T(8,128)(2,1)} %multiply_convert_fusion.refs_0_), channel_id=1, source_target_pairs={{0,1},{1,0},{2,3},{3,2},{4,5},{5,4},{6,7},{7,6},{8,9},{9,8},{10,11... | collective-permute-start | bytes 6291464 | tf_op jit(solution)/shard_map/ppermute | solution.py:232
  563.6 80.5 %collective-permute-start.47 = (bf16[512,2048]{1,0:T(8,128)(2,1)}, bf16[512,2048]{1,0:T(8,128)(2,1)}, u32[]{:S(2)}, u32[]{:S(2)}) collective-permute-start(bf16[512,2048]{1,0:T(8,128)(2,1)} %collective-permute-done.46.refs_0_), channel_id=1, source_target_pairs={{0,1},{1,0},{2,3},{3,2},{4,5},{5,4},{6,7},{7,6},{8,9},{9,8},{10,11... | collective-permute-start | bytes 6291464 | tf_op jit(solution)/shard_map/ppermute | solution.py:232
  606.3 75.2 %collective-permute-start.51 = (bf16[512,2048]{1,0:T(8,128)(2,1)}, bf16[512,2048]{1,0:T(8,128)(2,1)}, u32[]{:S(2)}, u32[]{:S(2)}) collective-permute-start(bf16[512,2048]{1,0:T(8,128)(2,1)} %collective-permute-done.50.refs_0_), channel_id=1, source_target_pairs={{0,1},{1,0},{2,3},{3,2},{4,5},{5,4},{6,7},{7,6},{8,9},{9,8},{10,11... | collective-permute-start | bytes 6291464 | tf_op jit(solution)/shard_map/ppermute | solution.py:232
  643.6 113.3 %collective-permute-start.44 = (bf16[512,2048]{1,0:T(8,128)(2,1)}, bf16[512,2048]{1,0:T(8,128)(2,1)}, u32[]{:S(2)}, u32[]{:S(2)}) collective-permute-start(bf16[512,2048]{1,0:T(8,128)(2,1)} %get-tuple-element.16), channel_id=1, source_target_pairs={{0,1},{1,0},{2,3},{3,2},{4,5},{5,4},{6,7},{7,6},{8,9},{9,8},{10,11... | collective-permute-start | bytes 6291464 | tf_op jit(solution)/shard_map/ppermute | solution.py:232
  681.5 78.6 %collective-permute-start.48 = (bf16[512,2048]{1,0:T(8,128)(2,1)}, bf16[512,2048]{1,0:T(8,128)(2,1)}, u32[]{:S(2)}, u32[]{:S(2)}) collective-permute-start(bf16[512,2048]{1,0:T(8,128)(2,1)} %get-tuple-element.18), channel_id=1, source_target_pairs={{0,1},{1,0},{2,3},{3,2},{4,5},{5,4},{6,7},{7,6},{8,9},{9,8},{10,11... | collective-permute-start | bytes 6291464 | tf_op jit(solution)/shard_map/ppermute | solution.py:232
  718.8 46.4 %collective-permute-start.52 = (bf16[512,2048]{1,0:T(8,128)(2,1)}, bf16[512,2048]{1,0:T(8,128)(2,1)}, u32[]{:S(2)}, u32[]{:S(2)}) collective-permute-start(bf16[512,2048]{1,0:T(8,128)(2,1)} %get-tuple-element.20), channel_id=1, source_target_pairs={{0,1},{1,0},{2,3},{3,2},{4,5},{5,4},{6,7},{7,6},{8,9},{9,8},{10,11... | collective-permute-start | bytes 6291464 | tf_op jit(solution)/shard_map/ppermute | solution.py:232
  760.0 87.7 %collective-permute-start.45 = (bf16[512,2048]{1,0:T(8,128)(2,1)S(1)}, bf16[512,2048]{1,0:T(8,128)(2,1)S(1)}, u32[]{:S(2)}, u32[]{:S(2)}) collective-permute-start(bf16[512,2048]{1,0:T(8,128)(2,1)S(1)} %add_convert_fusion.3), channel_id=1, source_target_pairs={{0,8},{2,10},{4,12},{6,14},{8,0},{10,2},{12,4},{14,6},{16,24},{18,... | collective-permute-start | bytes 6291464 | tf_op jit(solution)/shard_map/ppermute | solution.py:225
  762.6 138.4 %collective-permute-start.49 = (bf16[512,2048]{1,0:T(8,128)(2,1)S(1)}, bf16[512,2048]{1,0:T(8,128)(2,1)S(1)}, u32[]{:S(2)}, u32[]{:S(2)}) collective-permute-start(bf16[512,2048]{1,0:T(8,128)(2,1)S(1)} %add_convert_fusion.2), channel_id=1, source_target_pairs={{0,16},{2,18},{4,20},{6,22},{8,24},{10,26},{12,28},{14,30},{16,0},... | collective-permute-start | bytes 6291464 | tf_op jit(solution)/shard_map/ppermute | solution.py:225
  767.5 179.0 %collective-permute-start.53 = (bf16[512,2048]{1,0:T(8,128)(2,1)S(1)}, bf16[512,2048]{1,0:T(8,128)(2,1)S(1)}, u32[]{:S(2)}, u32[]{:S(2)}) collective-permute-start(bf16[512,2048]{1,0:T(8,128)(2,1)S(1)} %add_convert_fusion.1), channel_id=1, source_target_pairs={{0,24},{2,26},{4,28},{6,30},{8,16},{10,18},{12,20},{14,22},{16,8},... | collective-permute-start | bytes 6291464 | tf_op jit(solution)/shard_map/ppermute | solution.py:225
  (40 other events, 1253.8 us)

commit v2 on v1

--- a/solution.py
+++ b/solution.py
@@ -219,26 +219,28 @@
     )(part, col, squared, weight)
 
 
-def make_body(outer, inner, tp):
-    def swap_outer(value, k):
-        pairs = [(o * inner + i, (o ^ k) * inner + i) for o in range(outer) for i in range(inner)]
-        return lax.ppermute(value, "sp", pairs)
-
-    def swap_inner(value, r):
-        pairs = [(o * inner + i, o * inner + (i ^ r)) for o in range(outer) for i in range(inner)]
-        return lax.ppermute(value, "sp", pairs)
+def spread(index, bits):
+    return sum(((index >> n) & 1) << bit for n, bit in enumerate(bits))
+
+
+def make_body(sp, tp, near_bits, wide_bits):
+    near, wide = 1 << len(near_bits), 1 << len(wide_bits)
+    near_mask = [spread(c, near_bits) for c in range(near)]
+    wide_mask = [spread(m, wide_bits) for m in range(wide)]
+    groups = [[c] for c in range(1, near)]
+
+    def swap(value, mask):
+        return lax.ppermute(value, "sp", [(s, s ^ mask) for s in range(sp)])
 
     def swap_tp(value, j):
         return lax.ppermute(value, "tp", [(t, t ^ j) for t in range(tp)])
 
-    def gather_inner(value):
-        if inner != 4:
-            return [value] + [swap_inner(value, r) for r in range(1, inner)]
-        half = value.shape[0] // 2
-        first, second = swap_inner(value, 1), swap_inner(value, 2)
-        corner_a = swap_inner(second[:half], 1)
-        corner_b = swap_inner(first[half:], 2)
-        return [value, first, second, corner_a, corner_b]
+    def gather_wide(value):
+        if wide != 4:
+            return [value] + [swap(value, wide_mask[m]) for m in range(1, wide)]
+        high = swap(value, wide_mask[2])
+        low = swap(value, wide_mask[1])
+        return [value, low, high, swap(high, wide_mask[1])]
 
     def body(
         queries, keys, values, documents, query_gain, key_gain, residual, out_weight, norm_gain, up_weight, down_weight
@@ -247,34 +249,41 @@
         key_heads = keys.shape[1] // HD
         group = HQ // KV
         width = residual.shape[1]
-        sp_index = lax.axis_index("sp")
-        o, i, t = sp_index // inner, sp_index % inner, lax.axis_index("tp")
-        split = key_heads % outer == 0
-        units = up_weight.shape[1] // outer
+        here, t = lax.axis_index("sp"), lax.axis_index("tp")
+        own = sum(((here >> bit) & 1) << n for n, bit in enumerate(near_bits))
+        split = key_heads % near == 0
+        units = up_weight.shape[1] // near
         slab = up_weight.shape[0]
-        far = range(1, outer)
-        places = [(r, k) for r in range(inner) for k in (0,)] + [(r, k) for r in range(inner) for k in far]
+        far = range(1, near)
+        places = [(m, c) for cs in [[0]] + groups for m in range(wide) for c in cs]
         slots = len(places)
-        spots = jnp.stack([((o ^ k) * inner + (i ^ r)) * slab for r, k in places]).astype(jnp.int32)
+        spots = jnp.stack([(here ^ (wide_mask[m] ^ near_mask[c])) * slab for m, c in places]).astype(jnp.int32)
         part = (spots // width) ^ t.astype(jnp.int32)
         col = spots % width
 
-        docs_outer = jnp.stack([documents] + [swap_outer(documents, k) for k in far])
-        docs_all = jnp.concatenate([docs_outer] + [swap_inner(docs_outer, r) for r in range(1, inner)])
-
-        up_near = gather_inner(lax.dynamic_slice_in_dim(up_weight, o * units, units, 1))
-        down_near = gather_inner(lax.dynamic_slice_in_dim(down_weight, o * units, units, 0))
-        up_pieces = [swap_outer(lax.dynamic_slice_in_dim(up_weight, (o ^ k) * units, units, 1), k) for k in far]
-        down_pieces = [swap_outer(lax.dynamic_slice_in_dim(down_weight, (o ^ k) * units, units, 0), k) for k in far]
-        up_far = gather_inner(jnp.concatenate(up_pieces))
-        down_far = gather_inner(jnp.concatenate(down_pieces))
-
-        positions = sp_index * rows + jnp.arange(rows, dtype=jnp.int32)
+        def units_of(weight, c, axis):
+            return lax.dynamic_slice_in_dim(weight, (own ^ c) * units, units, axis)
+
+        def gather_units(weight, axis):
+            pieces = {c: swap(units_of(weight, c, axis), near_mask[c]) for c in far}
+            found = gather_wide(units_of(weight, 0, axis))
+            for cs in groups:
+                stacked = pieces[cs[0]] if len(cs) == 1 else jnp.concatenate([pieces[c] for c in cs])
+                found += gather_wide(stacked)
+            return jnp.concatenate(found)
+
+        up_whole = gather_units(up_weight, 1)
+        down_whole = gather_units(down_weight, 0)
+
+        docs_near = jnp.stack([documents] + [swap(documents, near_mask[c]) for c in far])
+        docs_all = jnp.concatenate([docs_near] + [swap(docs_near, wide_mask[m]) for m in range(1, wide)])
+
+        positions = here * rows + jnp.arange(rows, dtype=jnp.int32)
         queries_rot = grid_rotary(
             head_norm(queries.reshape(rows, key_heads * group, HD), query_gain), positions
         ).astype(jnp.bfloat16)
         keys_rot = grid_rotary(head_norm(keys.reshape(rows, key_heads, HD), key_gain), positions).astype(jnp.bfloat16)
-        parts = outer if split else 1
+        parts = near if split else 1
         heads = key_heads // parts
         q_width = heads * group * HD
         packed = jnp.concatenate(
@@ -287,17 +296,17 @@
         )
         packed = jnp.transpose(packed, (1, 0, 2))
         if split:
-            taken = [lax.dynamic_index_in_dim(packed, o ^ k, 0, keepdims=False) for k in range(outer)]
-            taken = [taken[0]] + [swap_outer(taken[k], k) for k in far]
+            taken = [lax.dynamic_index_in_dim(packed, own ^ c, 0, keepdims=False) for c in range(near)]
+            taken = [taken[0]] + [swap(taken[c], near_mask[c]) for c in far]
             q_blocks = jnp.stack([piece[:, :q_width] for piece in taken])
             kv_own = jnp.concatenate([piece[:, q_width:] for piece in taken])
-            q_docs = docs_outer
+            q_docs = docs_near
         else:
             q_blocks = packed[:, :, :q_width]
             kv_mine = packed[0, :, q_width:]
-            kv_own = jnp.concatenate([kv_mine] + [swap_outer(kv_mine, k) for k in far])
+            kv_own = jnp.concatenate([kv_mine] + [swap(kv_mine, near_mask[c]) for c in far])
             q_docs = documents[None]
-        kv_all = jnp.concatenate(gather_inner(kv_own)).reshape(outer * inner, rows, -1)
+        kv_all = jnp.concatenate(gather_wide(kv_own)).reshape(near * wide, rows, -1)
 
         attended = []
         for h in range(heads):
@@ -310,10 +319,10 @@
             attended.append(attend(q_head, kv_head, q_docs, docs_all, group))
         attended = attended[0] if heads == 1 else jnp.concatenate(attended, -1)
         if split:
-            merged = jnp.zeros((rows, outer * q_width), jnp.bfloat16)
-            for k in range(outer):
-                piece = attended[k] if k == 0 else swap_outer(attended[k], k)
-                merged = lax.dynamic_update_slice_in_dim(merged, piece, (o ^ k) * q_width, 1)
+            merged = jnp.zeros((rows, near * q_width), jnp.bfloat16)
+            for c in range(near):
+                piece = attended[c] if c == 0 else swap(attended[c], near_mask[c])
+                merged = lax.dynamic_update_slice_in_dim(merged, piece, (own ^ c) * q_width, 1)
             attended = merged
         else:
             attended = attended[0]
@@ -332,35 +341,35 @@
         normed = stream * lax.rsqrt(total_squares / (width * tp) + norm_eps)[:, None]
         normed = (normed * gain_here).astype(jnp.bfloat16)
 
-        up_whole = jnp.concatenate(up_near + up_far)
-        down_whole = jnp.concatenate(down_near + down_far)
-
+        chunks = [normed] * near
+        for c in far:
+            low = c & -c
+            via = chunks[c ^ low] if c != low else normed
+            chunks[c] = swap(via, near_mask[low])
         squared = []
-        for k in range(outer):
-            chunk = normed if k == 0 else swap_outer(normed, k)
-            chunk_parts = [chunk]
-            for j in range(1, tp):
-                chunk_parts.append(swap_tp(chunk, j))
+        for c in range(near):
+            chunk_parts = [chunks[c]] + [swap_tp(chunks[c], j) for j in range(1, tp)]
             squared.append(up_project(part, col, chunk_parts, up_whole, slots))
-        feed = [None] * outer
-        for k in list(far)[::-1] + [0]:
-            pieces = down_project(part, col, squared[k], down_whole, tp, slots)
+        feed = [None] * near
+        for c in list(far)[::-1] + [0]:
+            pieces = down_project(part, col, squared[c], down_whole, tp, slots)
             total = pieces[0].astype(jnp.float32)
             for j in range(1, tp):
                 total = total + swap_tp(pieces[j], j).astype(jnp.float32)
-            feed[k] = total if k == 0 else swap_outer(total.astype(jnp.bfloat16), k)
-        result = stream
-        for k in range(outer):
-            result = result + feed[k].astype(jnp.float32)
-        return result.astype(jnp.bfloat16)
+            feed[c] = total
+        for c in list(far)[::-1]:
+            low = c & -c
+            arrived = swap(feed[c].astype(jnp.bfloat16), near_mask[low])
+            feed[c ^ low] = feed[c ^ low] + arrived.astype(jnp.float32)
+        return (stream + feed[0]).astype(jnp.bfloat16)
 
     return body
 
 
 def solution(mesh):
     sp, tp = mesh.shape["sp"], mesh.shape["tp"]
-    outer = 1 << (sp.bit_length() // 2)
-    inner = sp // outer
+    bits = range(sp.bit_length() - 1)
+    near_bits, wide_bits = bits[0::2], bits[1::2]
     in_specs = (
         P("sp", "tp"),
         P("sp", "tp"),
@@ -375,5 +384,5 @@
         P("tp", "sp"),
     )
     return jax.shard_map(
-        make_body(outer, inner, tp), mesh=mesh, in_specs=in_specs, out_specs=P("sp", "tp"), check_vma=False
-    )
+        make_body(sp, tp, near_bits, wide_bits), mesh=mesh, in_specs=in_specs, out_specs=P("sp", "tp"), check_vma=False
+    )

time: 967 us -> 879 us (0.909)
  the two profiles are of different devices: /device:TPU:10 before, /device:TPU:0 now
where the time goes in v2:
time: 879 us; the launch traced here: 871 us
  waiting for transfers between devices  486 us (55%)
  Pallas kernels  193 us (22%)
  local copies, waits for them, and re-layouts  82.1 us (9%)
  starting transfers between devices  70.6 us (8%)
  other arithmetic  29.9 us (3%)
    ppermute x51, waiting for transfers between devices, swap(): return lax.ppermute(value, 'sp', [(s, s ^ mask) for s in range(sp)])  486 us
    pallas_call x4, Pallas kernels, down_project(): pl.pallas_call(functools.partial(down_kernel, slab=slab), grid_spec=grid_...  82 us
    ppermute x51, starting transfers between devices, swap(): return lax.ppermute(value, 'sp', [(s, s ^ mask) for s in range(sp)])  69.4 us
    pallas_call x4, Pallas kernels, up_project(): pl.pallas_call(functools.partial(up_kernel, tp=tp, slots=slots, slab=dept...  67.4 us
    unnamed x66, local copies, waits for them, and re-layouts  45.2 us
    pallas_call x1, Pallas kernels, attend(): pl.pallas_call(functools.partial(attend_kernel, group=group, blocks=block...  43.4 us
  transfers between devices with their start and end apart: 61, of which 29 were waited for; matrix products, arithmetic and copies ran while one was open for 11% of the time, Pallas kernels for 17%

profile of v2, /device:TPU:0, one launch (start us, length us, event | category | flops | bytes accessed | tf_op | source)
XLA Modules:
  0.0 870.5 jit_solution(6816266120535509009)
XLA Ops:
  17.8 7.3 collective-permute-done.6
  30.8 8.8 %collective-permute-done.8 = bf16[512,512]{1,0:T(8,128)(2,1)S(1)} collective-permute-done((bf16[512,512]{1,0:T(8,128)(2,1)S(1)}, bf16[512,512]{1,0:T(8,128)(2,1)S(1)}, u32[]{:S(2)}, u32[]{:S(2)}) %collective-permute-start.8) | collective-permute-done | bytes 524320 | tf_op jit(solution)/shard_map/ppermute | solution.py:233
  48.4 16.3 %collective-permute-done.1 = s32[512]{0:T(512)S(1)} collective-permute-done((s32[512]{0:T(512)S(1)}, s32[512]{0:T(512)S(1)}, u32[]{:S(2)}, u32[]{:S(2)}) %collective-permute-start.1) | collective-permute-done | bytes 2080 | tf_op jit(solution)/shard_map/ppermute | solution.py:233
  69.9 18.6 %collective-permute-done.10 = bf16[2048,256]{1,0:T(8,128)(2,1)S(1)} collective-permute-done((bf16[2048,256]{1,0:T(8,128)(2,1)S(1)}, bf16[2048,256]{1,0:T(8,128)(2,1)S(1)}, u32[]{:S(2)}, u32[]{:S(2)}) %collective-permute-start.10) | collective-permute-done | bytes 1048608 | tf_op jit(solution)/shard_map/ppermute | solution.py:233
  98.5 14.1 %collective-permute-done.11 = bf16[2048,256]{1,0:T(8,128)(2,1)} collective-permute-done((bf16[2048,256]{1,0:T(8,128)(2,1)S(1)}, bf16[2048,256]{1,0:T(8,128)(2,1)}, u32[]{:S(2)}, u32[]{:S(2)}) %collective-permute-start.11) | collective-permute-done | bytes 1048608 | tf_op jit(solution)/shard_map/ppermute | solution.py:233
  114.9 43.4 %attend.1 = bf16[2048,256]{1,0:T(8,128)(2,1)} custom-call(s32[128]{0:T(128)} %select_n.98.flags, bf16[2048,256]{1,0:T(8,128)(2,1)} %bitcast.54, bf16[16,512,256]{2,1,0:T(8,128)(2,1)} %bitcast.57, s32[8,1,512]{2,1,0:T(1,128)} %tile.8.qdoc_ref, s32[16,512,1]{2,1,0:T(8,128)} %copy.83.kdoc_ref), custom_call_target="tpu_custom_call" | custom-call | flops 8589934592 | bytes 6291456 | tf_op jit(solution)/shard_map/attend/pallas_call | solution.py:136
  168.0 16.5 %collective-permute-start.33 = (bf16[2048,256]{1,0:T(8,128)(2,1)S(1)}, bf16[2048,256]{1,0:T(8,128)(2,1)}, u32[]{:S(2)}, u32[]{:S(2)}) collective-permute-start(bf16[2048,256]{1,0:T(8,128)(2,1)S(1)} %get-tuple-element.30), channel_id=1, source_target_pairs={{0,4},{2,6},{4,0},{6,2},{8,12},{10,14},{12,8},{14,10},{16,20},{18,... | collective-permute-start | bytes 3145736 | tf_op jit(solution)/shard_map/ppermute | solution.py:233
  189.5 8.2 convolution_convert_fusion
  209.5 45.0 %collective-permute-done.34 = bf16[2048,256]{1,0:T(8,128)(2,1)S(1)} collective-permute-done((bf16[2048,256]{1,0:T(8,128)(2,1)S(1)}, bf16[2048,256]{1,0:T(8,128)(2,1)S(1)}, u32[]{:S(2)}, u32[]{:S(2)}) %collective-permute-start.34) | collective-permute-done | bytes 1048608 | tf_op jit(solution)/shard_map/ppermute | solution.py:233
  263.5 13.1 %collective-permute-done.19 = bf16[256,2048]{1,0:T(8,128)(2,1)} collective-permute-done((bf16[256,2048]{1,0:T(8,128)(2,1)}, bf16[256,2048]{1,0:T(8,128)(2,1)}, u32[]{:S(2)}, u32[]{:S(2)}) %collective-permute-start.19) | collective-permute-done | bytes 1048608 | tf_op jit(solution)/shard_map/ppermute | solution.py:233
  282.0 17.0 %collective-permute-done.40 = bf16[2048,256]{1,0:T(8,128)(2,1)} collective-permute-done((bf16[2048,256]{1,0:T(8,128)(2,1)}, bf16[2048,256]{1,0:T(8,128)(2,1)}, u32[]{:S(2)}, u32[]{:S(2)}) %collective-permute-start.40) | collective-permute-done | bytes 1048608 | tf_op jit(solution)/shard_map/ppermute | solution.py:233
  305.1 16.6 %collective-permute-done.44 = bf16[2048,256]{1,0:T(8,128)(2,1)S(1)} collective-permute-done((bf16[2048,256]{1,0:T(8,128)(2,1)S(1)}, bf16[2048,256]{1,0:T(8,128)(2,1)S(1)}, u32[]{:S(2)}, u32[]{:S(2)}) %collective-permute-start.44) | collective-permute-done | bytes 1048608 | tf_op jit(solution)/shard_map/ppermute | solution.py:233
  329.0 34.6 %collective-permute-done.25 = bf16[256,2048]{1,0:T(8,128)(2,1)S(1)} collective-permute-done((bf16[256,2048]{1,0:T(8,128)(2,1)S(1)}, bf16[256,2048]{1,0:T(8,128)(2,1)S(1)}, u32[]{:S(2)}, u32[]{:S(2)}) %collective-permute-start.25) | collective-permute-done | bytes 1048608 | tf_op jit(solution)/shard_map/ppermute | solution.py:233
  363.6 23.4 %collective-permute-done.29 = bf16[256,2048]{1,0:T(8,128)(2,1)S(1)} collective-permute-done((bf16[256,2048]{1,0:T(8,128)(2,1)S(1)}, bf16[256,2048]{1,0:T(8,128)(2,1)S(1)}, u32[]{:S(2)}, u32[]{:S(2)}) %collective-permute-start.29) | collective-permute-done | bytes 1048608 | tf_op jit(solution)/shard_map/ppermute | solution.py:233
  391.4 26.9 %collective-permute-done.38 = bf16[2048,256]{1,0:T(8,128)(2,1)S(1)} collective-permute-done((bf16[2048,256]{1,0:T(8,128)(2,1)}, bf16[2048,256]{1,0:T(8,128)(2,1)S(1)}, u32[]{:S(2)}, u32[]{:S(2)}) %collective-permute-start.38) | collective-permute-done | bytes 1048608 | tf_op jit(solution)/shard_map/ppermute | solution.py:233
  418.6 22.3 %collective-permute-done.42 = bf16[2048,256]{1,0:T(8,128)(2,1)S(1)} collective-permute-done((bf16[2048,256]{1,0:T(8,128)(2,1)}, bf16[2048,256]{1,0:T(8,128)(2,1)S(1)}, u32[]{:S(2)}, u32[]{:S(2)}) %collective-permute-start.42) | collective-permute-done | bytes 1048608 | tf_op jit(solution)/shard_map/ppermute | solution.py:233
  448.4 12.6 %collective-permute-done.23 = bf16[256,2048]{1,0:T(8,128)(2,1)S(1)} collective-permute-done((bf16[256,2048]{1,0:T(8,128)(2,1)S(1)}, bf16[256,2048]{1,0:T(8,128)(2,1)S(1)}, u32[]{:S(2)}, u32[]{:S(2)}) %collective-permute-start.23) | collective-permute-done | bytes 1048608 | tf_op jit(solution)/shard_map/ppermute | solution.py:233
  471.8 20.0 %collective-permute-done.45 = bf16[2048,256]{1,0:T(8,128)(2,1)S(1)} collective-permute-done((bf16[2048,256]{1,0:T(8,128)(2,1)S(1)}, bf16[2048,256]{1,0:T(8,128)(2,1)S(1)}, u32[]{:S(2)}, u32[]{:S(2)}) %collective-permute-start.45) | collective-permute-done | bytes 1048608 | tf_op jit(solution)/shard_map/ppermute | solution.py:233
  494.3 32.9 %collective-permute-done.49.refs_0_ = bf16[512,2048]{1,0:T(8,128)(2,1)S(1)} collective-permute-done((bf16[512,2048]{1,0:T(8,128)(2,1)}, bf16[512,2048]{1,0:T(8,128)(2,1)S(1)}, u32[]{:S(2)}, u32[]{:S(2)}) %collective-permute-start.49) | collective-permute-done | bytes 2097184 | tf_op jit(solution)/shard_map/ppermute | solution.py:233
  538.0 39.6 %collective-permute-done.27 = bf16[256,2048]{1,0:T(8,128)(2,1)S(1)} collective-permute-done((bf16[256,2048]{1,0:T(8,128)(2,1)S(1)}, bf16[256,2048]{1,0:T(8,128)(2,1)S(1)}, u32[]{:S(2)}, u32[]{:S(2)}) %collective-permute-start.27) | collective-permute-done | bytes 1048608 | tf_op jit(solution)/shard_map/ppermute | solution.py:233
  584.1 12.9 %collective-permute-done.31 = bf16[256,2048]{1,0:T(8,128)(2,1)S(1)} collective-permute-done((bf16[256,2048]{1,0:T(8,128)(2,1)S(1)}, bf16[256,2048]{1,0:T(8,128)(2,1)S(1)}, u32[]{:S(2)}, u32[]{:S(2)}) %collective-permute-start.31) | collective-permute-done | bytes 1048608 | tf_op jit(solution)/shard_map/ppermute | solution.py:233
  606.4 18.1 %collective-permute-done.47 = bf16[2048,256]{1,0:T(8,128)(2,1)S(1)} collective-permute-done((bf16[2048,256]{1,0:T(8,128)(2,1)S(1)}, bf16[2048,256]{1,0:T(8,128)(2,1)S(1)}, u32[]{:S(2)}, u32[]{:S(2)}) %collective-permute-start.47) | collective-permute-done | bytes 1048608 | tf_op jit(solution)/shard_map/ppermute | solution.py:233
  625.5 19.4 %collective-permute-done.32 = bf16[256,2048]{1,0:T(8,128)(2,1)S(1)} collective-permute-done((bf16[256,2048]{1,0:T(8,128)(2,1)S(1)}, bf16[256,2048]{1,0:T(8,128)(2,1)S(1)}, u32[]{:S(2)}, u32[]{:S(2)}) %collective-permute-start.32) | collective-permute-done | bytes 1048608 | tf_op jit(solution)/shard_map/ppermute | solution.py:233
  647.9 16.8 %shard_map.111.x_ref = bf16[512,2048]{1,0:T(8,128)(2,1)} custom-call(s32[16]{0:T(128)} %get-tuple-element.72.part, s32[16]{0:T(128)} %get-tuple-element.71.col, bf16[512,2048]{1,0:T(8,128)(2,1)} %copy-done.14, bf16[512,2048]{1,0:T(8,128)(2,1)} %copy-done.15, bf16[4096,2048]{1,0:T(8,128)(2,1)} %constant_dynamic-update-slice_fusion.8.refs_2_), custom_call_target="tpu_custom_call" | custom-call | flops 8589934592 | bytes 20971520 | tf_op jit(solution)/shard_map/pallas_call | solution.py:179
  664.7 16.8 %shard_map.113.x_ref = bf16[512,2048]{1,0:T(8,128)(2,1)} custom-call(s32[16]{0:T(128)} %get-tuple-element.72.part, s32[16]{0:T(128)} %get-tuple-element.71.col, bf16[512,2048]{1,0:T(8,128)(2,1)} %collective-permute-done.52.refs_0_, bf16[512,2048]{1,0:T(8,128)(2,1)} %collective-permute-done.53.refs_1_, ...), custom_call_target="tpu_custom_call" | custom-call | flops 8589934592 | bytes 20971520 | tf_op jit(solution)/shard_map/pallas_call | solution.py:179
  681.5 20.5 %shard_map.114 = (bf16[512,2048]{1,0:T(8,128)(2,1)}, bf16[512,2048]{1,0:T(8,128)(2,1)}) custom-call(s32[16]{0:T(128)} %get-tuple-element.72.part, s32[16]{0:T(128)} %get-tuple-element.71.col, bf16[512,2048]{1,0:T(8,128)(2,1)} %shard_map.113.x_ref, bf16[32768,256]{1,0:T(8,128)(2,1)} %constant_dynamic-update-slice_fusion.24.w_ref), custom_call_target="tpu_custom_call" | custom-call | flops 8589934592 | bytes 18874368 | tf_op jit(solution)/shard_map/pallas_call | solution.py:212
  702.0 20.5 %shard_map.112 = (bf16[512,2048]{1,0:T(8,128)(2,1)}, bf16[512,2048]{1,0:T(8,128)(2,1)}) custom-call(s32[16]{0:T(128)} %get-tuple-element.72.part, s32[16]{0:T(128)} %get-tuple-element.71.col, bf16[512,2048]{1,0:T(8,128)(2,1)} %shard_map.111.x_ref, bf16[32768,256]{1,0:T(8,128)(2,1)} %constant_dynamic-update-slice_fusion.24.w_ref), custom_call_target="tpu_custom_call" | custom-call | flops 8589934592 | bytes 18874368 | tf_op jit(solution)/shard_map/pallas_call | solution.py:212
  723.0 16.8 %shard_map.115.x_ref = bf16[512,2048]{1,0:T(8,128)(2,1)} custom-call(s32[16]{0:T(128)} %get-tuple-element.72.part, s32[16]{0:T(128)} %get-tuple-element.71.col, bf16[512,2048]{1,0:T(8,128)(2,1)} %collective-permute-done.57.refs_0_, bf16[512,2048]{1,0:T(8,128)(2,1)} %collective-permute-done.58.refs_1_, ...), custom_call_target="tpu_custom_call" | custom-call | flops 8589934592 | bytes 20971520 | tf_op jit(solution)/shard_map/pallas_call | solution.py:179
  739.8 20.5 %shard_map.116 = (bf16[512,2048]{1,0:T(8,128)(2,1)}, bf16[512,2048]{1,0:T(8,128)(2,1)}) custom-call(s32[16]{0:T(128)} %get-tuple-element.72.part, s32[16]{0:T(128)} %get-tuple-element.71.col, bf16[512,2048]{1,0:T(8,128)(2,1)} %shard_map.115.x_ref, bf16[32768,256]{1,0:T(8,128)(2,1)} %constant_dynamic-update-slice_fusion.24.w_ref), custom_call_target="tpu_custom_call" | custom-call | flops 8589934592 | bytes 18874368 | tf_op jit(solution)/shard_map/pallas_call | solution.py:212
  765.1 17.0 %shard_map.109.x_ref = bf16[512,2048]{1,0:T(8,128)(2,1)} custom-call(s32[16]{0:T(128)} %get-tuple-element.72.part, s32[16]{0:T(128)} %get-tuple-element.71.col, bf16[512,2048]{1,0:T(8,128)(2,1)} %multiply_convert_fusion.refs_0_, bf16[512,2048]{1,0:T(8,128)(2,1)} %collective-permute-done.17.refs_1_, bf16[4096,2048]{1,0:T(8,128)(2,1)} %constant_dynamic-update-slice_fusion.8.refs_2_), custom_call_target="tpu_custom_call" | custom-call | flops 8589934592 | bytes 20971520 | tf_op jit(solution)/shard_map/pallas_call | solution.py:179
  782.1 20.5 %shard_map.110 = (bf16[512,2048]{1,0:T(8,128)(2,1)}, bf16[512,2048]{1,0:T(8,128)(2,1)}) custom-call(s32[16]{0:T(128)} %get-tuple-element.72.part, s32[16]{0:T(128)} %get-tuple-element.71.col, bf16[512,2048]{1,0:T(8,128)(2,1)} %shard_map.109.x_ref, bf16[32768,256]{1,0:T(8,128)(2,1)} %constant_dynamic-update-slice_fusion.24.w_ref), custom_call_target="tpu_custom_call" | custom-call | flops 8589934592 | bytes 18874368 | tf_op jit(solution)/shard_map/pallas_call | solution.py:212
  817.4 40.5 %collective-permute-done.60 = bf16[512,2048]{1,0:T(8,128)(2,1)S(1)} collective-permute-done((bf16[512,2048]{1,0:T(8,128)(2,1)S(1)}, bf16[512,2048]{1,0:T(8,128)(2,1)S(1)}, u32[]{:S(2)}, u32[]{:S(2)}) %collective-permute-start.60) | collective-permute-done | bytes 2097184 | tf_op jit(solution)/shard_map/ppermute | solution.py:233
  (229 shorter events, 192.3 us)
Async XLA Ops:
  43.3 53.0 %collective-permute-start.9 = (bf16[2048,256]{1,0:T(8,128)(2,1)S(1)}, bf16[2048,256]{1,0:T(8,128)(2,1)S(1)}, u32[]{:S(2)}, u32[]{:S(2)}) collective-permute-start(bf16[2048,256]{1,0:T(8,128)(2,1)S(1)} %pad_maximum_fusion.2), channel_id=1, source_target_pairs={{0,4},{2,6},{4,0},{6,2},{8,12},{10,14},{12,8},{14,10},{16,20},{18,... | collective-permute-start | bytes 3145736 | tf_op jit(solution)/shard_map/ppermute | solution.py:233
  184.5 70.0 %collective-permute-start.34 = (bf16[2048,256]{1,0:T(8,128)(2,1)S(1)}, bf16[2048,256]{1,0:T(8,128)(2,1)S(1)}, u32[]{:S(2)}, u32[]{:S(2)}) collective-permute-start(bf16[2048,256]{1,0:T(8,128)(2,1)S(1)} %get-tuple-element.30), channel_id=1, source_target_pairs={{0,16},{2,18},{4,20},{6,22},{8,24},{10,26},{12,28},{14,30},{16,0},... | collective-permute-start | bytes 3145736 | tf_op jit(solution)/shard_map/ppermute | solution.py:233
  199.2 99.8 %collective-permute-start.15 = (bf16[512,2048]{1,0:T(8,128)(2,1)}, bf16[512,2048]{1,0:T(8,128)(2,1)}, u32[]{:S(2)}, u32[]{:S(2)}) collective-permute-start(bf16[512,2048]{1,0:T(8,128)(2,1)} %constant_dynamic-slice_fusion.8), channel_id=1, source_target_pairs={{0,1},{1,0},{2,3},{3,2},{4,5},{5,4},{6,7},{7,6},{8,9},{9,8},{10,11... | collective-permute-start | bytes 6291464 | tf_op jit(solution)/shard_map/ppermute | solution.py:236
  199.2 58.7 %collective-permute-start.36 = (bf16[2048,256]{1,0:T(8,128)(2,1)}, bf16[2048,256]{1,0:T(8,128)(2,1)}, u32[]{:S(2)}, u32[]{:S(2)}) collective-permute-start(bf16[2048,256]{1,0:T(8,128)(2,1)} %get-tuple-element.28), channel_id=1, source_target_pairs={{0,2},{2,0},{4,6},{6,4},{8,10},{10,8},{12,14},{14,12},{16,18},{18,... | collective-permute-start | bytes 3145736 | tf_op jit(solution)/shard_map/ppermute | solution.py:233
  204.6 56.4 %collective-permute-start.18 = (bf16[256,2048]{1,0:T(8,128)(2,1)}, bf16[256,2048]{1,0:T(8,128)(2,1)}, u32[]{:S(2)}, u32[]{:S(2)}) collective-permute-start(bf16[256,2048]{1,0:T(8,128)(2,1)} %get-tuple-element.35), channel_id=1, source_target_pairs={{0,4},{2,6},{4,0},{6,2},{8,12},{10,14},{12,8},{14,10},{16,20},{18,... | collective-permute-start | bytes 3145736 | tf_op jit(solution)/shard_map/ppermute | solution.py:233
  209.4 67.2 %collective-permute-start.19 = (bf16[256,2048]{1,0:T(8,128)(2,1)}, bf16[256,2048]{1,0:T(8,128)(2,1)}, u32[]{:S(2)}, u32[]{:S(2)}) collective-permute-start(bf16[256,2048]{1,0:T(8,128)(2,1)} %get-tuple-element.35), channel_id=1, source_target_pairs={{0,16},{2,18},{4,20},{6,22},{8,24},{10,26},{12,28},{14,30},{16,0},... | collective-permute-start | bytes 3145736 | tf_op jit(solution)/shard_map/ppermute | solution.py:233
  261.0 60.7 %collective-permute-start.44 = (bf16[2048,256]{1,0:T(8,128)(2,1)S(1)}, bf16[2048,256]{1,0:T(8,128)(2,1)S(1)}, u32[]{:S(2)}, u32[]{:S(2)}) collective-permute-start(bf16[2048,256]{1,0:T(8,128)(2,1)S(1)} %get-tuple-element.27), channel_id=1, source_target_pairs={{0,10},{2,8},{4,14},{6,12},{8,2},{10,0},{12,6},{14,4},{16,26},{18,... | collective-permute-start | bytes 3145736 | tf_op jit(solution)/shard_map/ppermute | solution.py:233
  299.1 64.5 %collective-permute-start.25 = (bf16[256,2048]{1,0:T(8,128)(2,1)S(1)}, bf16[256,2048]{1,0:T(8,128)(2,1)S(1)}, u32[]{:S(2)}, u32[]{:S(2)}) collective-permute-start(bf16[256,2048]{1,0:T(8,128)(2,1)S(1)} %copy-done.8), channel_id=1, source_target_pairs={{0,8},{2,10},{4,12},{6,14},{8,0},{10,2},{12,4},{14,6},{16,24},{18,... | collective-permute-start | bytes 3145736 | tf_op jit(solution)/shard_map/ppermute | solution.py:233
  299.1 87.8 %collective-permute-start.29 = (bf16[256,2048]{1,0:T(8,128)(2,1)S(1)}, bf16[256,2048]{1,0:T(8,128)(2,1)S(1)}, u32[]{:S(2)}, u32[]{:S(2)}) collective-permute-start(bf16[256,2048]{1,0:T(8,128)(2,1)S(1)} %copy-done.7), channel_id=1, source_target_pairs={{0,10},{2,8},{4,14},{6,12},{8,2},{10,0},{12,6},{14,4},{16,26},{18,... | collective-permute-start | bytes 3145736 | tf_op jit(solution)/shard_map/ppermute | solution.py:233
  321.7 69.7 %collective-permute-start.37 = (bf16[2048,256]{1,0:T(8,128)(2,1)}, bf16[2048,256]{1,0:T(8,128)(2,1)S(1)}, u32[]{:S(2)}, u32[]{:S(2)}) collective-permute-start(bf16[2048,256]{1,0:T(8,128)(2,1)} %collective-permute-done.36), channel_id=1, source_target_pairs={{0,4},{2,6},{4,0},{6,2},{8,12},{10,14},{12,8},{14,10},{16,20},{18,... | collective-permute-start | bytes 3145736 | tf_op jit(solution)/shard_map/ppermute | solution.py:233
  323.8 94.6 %collective-permute-start.38 = (bf16[2048,256]{1,0:T(8,128)(2,1)}, bf16[2048,256]{1,0:T(8,128)(2,1)S(1)}, u32[]{:S(2)}, u32[]{:S(2)}) collective-permute-start(bf16[2048,256]{1,0:T(8,128)(2,1)} %collective-permute-done.36), channel_id=1, source_target_pairs={{0,16},{2,18},{4,20},{6,22},{8,24},{10,26},{12,28},{14,30},{16,0},... | collective-permute-start | bytes 3145736 | tf_op jit(solution)/shard_map/ppermute | solution.py:233
  323.8 117.1 %collective-permute-start.42 = (bf16[2048,256]{1,0:T(8,128)(2,1)}, bf16[2048,256]{1,0:T(8,128)(2,1)S(1)}, u32[]{:S(2)}, u32[]{:S(2)}) collective-permute-start(bf16[2048,256]{1,0:T(8,128)(2,1)} %collective-permute-done.40), channel_id=1, source_target_pairs={{0,16},{2,18},{4,20},{6,22},{8,24},{10,26},{12,28},{14,30},{16,0},... | collective-permute-start | bytes 3145736 | tf_op jit(solution)/shard_map/ppermute | solution.py:233
  363.5 79.5 %collective-permute-start.20 = (bf16[256,2048]{1,0:T(8,128)(2,1)}, bf16[256,2048]{1,0:T(8,128)(2,1)S(1)}, u32[]{:S(2)}, u32[]{:S(2)}) collective-permute-start(bf16[256,2048]{1,0:T(8,128)(2,1)} %collective-permute-done.19), channel_id=1, source_target_pairs={{0,4},{2,6},{4,0},{6,2},{8,12},{10,14},{12,8},{14,10},{16,20},{18,... | collective-permute-start | bytes 3145736 | tf_op jit(solution)/shard_map/ppermute | solution.py:233
  386.9 57.4 %collective-permute-start.22 = (bf16[256,2048]{1,0:T(8,128)(2,1)S(1)}, bf16[256,2048]{1,0:T(8,128)(2,1)S(1)}, u32[]{:S(2)}, u32[]{:S(2)}) collective-permute-start(bf16[256,2048]{1,0:T(8,128)(2,1)S(1)} %collective-permute-done.21), channel_id=1, source_target_pairs={{0,4},{2,6},{4,0},{6,2},{8,12},{10,14},{12,8},{14,10},{16,20},{18,... | collective-permute-start | bytes 3145736 | tf_op jit(solution)/shard_map/ppermute | solution.py:233
  391.4 69.6 %collective-permute-start.23 = (bf16[256,2048]{1,0:T(8,128)(2,1)S(1)}, bf16[256,2048]{1,0:T(8,128)(2,1)S(1)}, u32[]{:S(2)}, u32[]{:S(2)}) collective-permute-start(bf16[256,2048]{1,0:T(8,128)(2,1)S(1)} %collective-permute-done.21), channel_id=1, source_target_pairs={{0,16},{2,18},{4,20},{6,22},{8,24},{10,26},{12,28},{14,30},{16,0},... | collective-permute-start | bytes 3145736 | tf_op jit(solution)/shard_map/ppermute | solution.py:233
  440.9 86.4 %collective-permute-start.49 = (bf16[512,2048]{1,0:T(8,128)(2,1)}, bf16[512,2048]{1,0:T(8,128)(2,1)S(1)}, u32[]{:S(2)}, u32[]{:S(2)}) collective-permute-start(bf16[512,2048]{1,0:T(8,128)(2,1)} %multiply_convert_fusion.refs_0_), channel_id=1, source_target_pairs={{0,8},{2,10},{4,12},{6,14},{8,0},{10,2},{12,4},{14,6},{16,24},{18,... | collective-permute-start | bytes 6291464 | tf_op jit(solution)/shard_map/ppermute | solution.py:233
  461.0 71.7 %collective-permute-start.46 = (bf16[2048,256]{1,0:T(8,128)(2,1)S(1)}, bf16[2048,256]{1,0:T(8,128)(2,1)S(1)}, u32[]{:S(2)}, u32[]{:S(2)}) collective-permute-start(bf16[2048,256]{1,0:T(8,128)(2,1)S(1)} %collective-permute-done.44), channel_id=1, source_target_pairs={{0,16},{2,18},{4,20},{6,22},{8,24},{10,26},{12,28},{14,30},{16,0},... | collective-permute-start | bytes 3145736 | tf_op jit(solution)/shard_map/ppermute | solution.py:233
  461.0 72.2 %collective-permute-start.43 = (bf16[2048,256]{1,0:T(8,128)(2,1)S(1)}, bf16[2048,256]{1,0:T(8,128)(2,1)S(1)}, u32[]{:S(2)}, u32[]{:S(2)}) collective-permute-start(bf16[2048,256]{1,0:T(8,128)(2,1)S(1)} %collective-permute-done.42), channel_id=1, source_target_pairs={{0,4},{2,6},{4,0},{6,2},{8,12},{10,14},{12,8},{14,10},{16,20},{18,... | collective-permute-start | bytes 3145736 | tf_op jit(solution)/shard_map/ppermute | solution.py:233
  469.3 67.6 %collective-permute-start.24 = (bf16[256,2048]{1,0:T(8,128)(2,1)S(1)}, bf16[256,2048]{1,0:T(8,128)(2,1)S(1)}, u32[]{:S(2)}, u32[]{:S(2)}) collective-permute-start(bf16[256,2048]{1,0:T(8,128)(2,1)S(1)} %collective-permute-done.23), channel_id=1, source_target_pairs={{0,4},{2,6},{4,0},{6,2},{8,12},{10,14},{12,8},{14,10},{16,20},{18,... | collective-permute-start | bytes 3145736 | tf_op jit(solution)/shard_map/ppermute | solution.py:233
  491.7 85.9 %collective-permute-start.27 = (bf16[256,2048]{1,0:T(8,128)(2,1)S(1)}, bf16[256,2048]{1,0:T(8,128)(2,1)S(1)}, u32[]{:S(2)}, u32[]{:S(2)}) collective-permute-start(bf16[256,2048]{1,0:T(8,128)(2,1)S(1)} %collective-permute-done.25), channel_id=1, source_target_pairs={{0,16},{2,18},{4,20},{6,22},{8,24},{10,26},{12,28},{14,30},{16,0},... | collective-permute-start | bytes 3145736 | tf_op jit(solution)/shard_map/ppermute | solution.py:233
  527.2 74.8 %collective-permute-start.52 = (bf16[512,2048]{1,0:T(8,128)(2,1)S(1)}, bf16[512,2048]{1,0:T(8,128)(2,1)}, u32[]{:S(2)}, u32[]{:S(2)}) collective-permute-start(bf16[512,2048]{1,0:T(8,128)(2,1)S(1)} %collective-permute-done.49.refs_0_), channel_id=1, source_target_pairs={{0,2},{2,0},{4,6},{6,4},{8,10},{10,8},{12,14},{14,12},{16,18},{18,... | collective-permute-start | bytes 6291464 | tf_op jit(solution)/shard_map/ppermute | solution.py:233
  533.2 48.7 %collective-permute-start.30 = (bf16[256,2048]{1,0:T(8,128)(2,1)S(1)}, bf16[256,2048]{1,0:T(8,128)(2,1)S(1)}, u32[]{:S(2)}, u32[]{:S(2)}) collective-permute-start(bf16[256,2048]{1,0:T(8,128)(2,1)S(1)} %collective-permute-done.29), channel_id=1, source_target_pairs={{0,4},{2,6},{4,0},{6,2},{8,12},{10,14},{12,8},{14,10},{16,20},{18,... | collective-permute-start | bytes 3145736 | tf_op jit(solution)/shard_map/ppermute | solution.py:233
  536.8 60.2 %collective-permute-start.31 = (bf16[256,2048]{1,0:T(8,128)(2,1)S(1)}, bf16[256,2048]{1,0:T(8,128)(2,1)S(1)}, u32[]{:S(2)}, u32[]{:S(2)}) collective-permute-start(bf16[256,2048]{1,0:T(8,128)(2,1)S(1)} %collective-permute-done.29), channel_id=1, source_target_pairs={{0,16},{2,18},{4,20},{6,22},{8,24},{10,26},{12,28},{14,30},{16,0},... | collective-permute-start | bytes 3145736 | tf_op jit(solution)/shard_map/ppermute | solution.py:233
  580.3 65.8 %collective-permute-start.57 = (bf16[512,2048]{1,0:T(8,128)(2,1)}, bf16[512,2048]{1,0:T(8,128)(2,1)}, u32[]{:S(2)}, u32[]{:S(2)}) collective-permute-start(bf16[512,2048]{1,0:T(8,128)(2,1)} %multiply_convert_fusion.refs_0_), channel_id=1, source_target_pairs={{0,2},{2,0},{4,6},{6,4},{8,10},{10,8},{12,14},{14,12},{16,18},{18,... | collective-permute-start | bytes 6291464 | tf_op jit(solution)/shard_map/ppermute | solution.py:233
  581.9 64.7 %collective-permute-start.50 = (bf16[512,2048]{1,0:T(8,128)(2,1)S(1)}, bf16[512,2048]{1,0:T(8,128)(2,1)S(1)}, u32[]{:S(2)}, u32[]{:S(2)}) collective-permute-start(bf16[512,2048]{1,0:T(8,128)(2,1)S(1)} %collective-permute-done.49.refs_0_), channel_id=1, source_target_pairs={{0,1},{1,0},{2,3},{3,2},{4,5},{5,4},{6,7},{7,6},{8,9},{9,8},{10,11... | collective-permute-start | bytes 6291464 | tf_op jit(solution)/shard_map/ppermute | solution.py:236
  602.0 62.7 %collective-permute-start.53 = (bf16[512,2048]{1,0:T(8,128)(2,1)}, bf16[512,2048]{1,0:T(8,128)(2,1)}, u32[]{:S(2)}, u32[]{:S(2)}) collective-permute-start(bf16[512,2048]{1,0:T(8,128)(2,1)} %collective-permute-done.52.refs_0_), channel_id=1, source_target_pairs={{0,1},{1,0},{2,3},{3,2},{4,5},{5,4},{6,7},{7,6},{8,9},{9,8},{10,11... | collective-permute-start | bytes 6291464 | tf_op jit(solution)/shard_map/ppermute | solution.py:236
  646.1 119.0 %collective-permute-start.17 = (bf16[512,2048]{1,0:T(8,128)(2,1)}, bf16[512,2048]{1,0:T(8,128)(2,1)}, u32[]{:S(2)}, u32[]{:S(2)}) collective-permute-start(bf16[512,2048]{1,0:T(8,128)(2,1)} %multiply_convert_fusion.refs_0_), channel_id=1, source_target_pairs={{0,1},{1,0},{2,3},{3,2},{4,5},{5,4},{6,7},{7,6},{8,9},{9,8},{10,11... | collective-permute-start | bytes 6291464 | tf_op jit(solution)/shard_map/ppermute | solution.py:236
  646.1 76.9 %collective-permute-start.58 = (bf16[512,2048]{1,0:T(8,128)(2,1)}, bf16[512,2048]{1,0:T(8,128)(2,1)}, u32[]{:S(2)}, u32[]{:S(2)}) collective-permute-start(bf16[512,2048]{1,0:T(8,128)(2,1)} %collective-permute-done.57.refs_0_), channel_id=1, source_target_pairs={{0,1},{1,0},{2,3},{3,2},{4,5},{5,4},{6,7},{7,6},{8,9},{9,8},{10,11... | collective-permute-start | bytes 6291464 | tf_op jit(solution)/shard_map/ppermute | solution.py:236
  702.0 58.3 %collective-permute-start.54 = (bf16[512,2048]{1,0:T(8,128)(2,1)}, bf16[512,2048]{1,0:T(8,128)(2,1)}, u32[]{:S(2)}, u32[]{:S(2)}) collective-permute-start(bf16[512,2048]{1,0:T(8,128)(2,1)} %get-tuple-element.18), channel_id=1, source_target_pairs={{0,1},{1,0},{2,3},{3,2},{4,5},{5,4},{6,7},{7,6},{8,9},{9,8},{10,11... | collective-permute-start | bytes 6291464 | tf_op jit(solution)/shard_map/ppermute | solution.py:236
  722.5 85.2 %collective-permute-start.51 = (bf16[512,2048]{1,0:T(8,128)(2,1)}, bf16[512,2048]{1,0:T(8,128)(2,1)}, u32[]{:S(2)}, u32[]{:S(2)}) collective-permute-start(bf16[512,2048]{1,0:T(8,128)(2,1)} %get-tuple-element.16), channel_id=1, source_target_pairs={{0,1},{1,0},{2,3},{3,2},{4,5},{5,4},{6,7},{7,6},{8,9},{9,8},{10,11... | collective-permute-start | bytes 6291464 | tf_op jit(solution)/shard_map/ppermute | solution.py:236
  764.8 48.8 %collective-permute-start.55 = (bf16[512,2048]{1,0:T(8,128)(2,1)}, bf16[512,2048]{1,0:T(8,128)(2,1)}, u32[]{:S(2)}, u32[]{:S(2)}) collective-permute-start(bf16[512,2048]{1,0:T(8,128)(2,1)} %add_convert_fusion.3), channel_id=1, source_target_pairs={{0,2},{2,0},{4,6},{6,4},{8,10},{10,8},{12,14},{14,12},{16,18},{18,... | collective-permute-start | bytes 6291464 | tf_op jit(solution)/shard_map/ppermute | solution.py:233
  805.9 52.0 %collective-permute-start.60 = (bf16[512,2048]{1,0:T(8,128)(2,1)S(1)}, bf16[512,2048]{1,0:T(8,128)(2,1)S(1)}, u32[]{:S(2)}, u32[]{:S(2)}) collective-permute-start(bf16[512,2048]{1,0:T(8,128)(2,1)S(1)} %add_convert_fusion.1), channel_id=1, source_target_pairs={{0,2},{2,0},{4,6},{6,4},{8,10},{10,8},{12,14},{14,12},{16,18},{18,... | collective-permute-start | bytes 6291464 | tf_op jit(solution)/shard_map/ppermute | solution.py:233
  (46 other events, 1350.4 us)

commit v3 on v2

--- a/solution.py
+++ b/solution.py
@@ -145,8 +145,9 @@
     return out.reshape(q_blocks.shape)
 
 
-def up_kernel(part, col, *refs, tp, slots, slab):
-    x_refs, w_ref, out_ref, rows_ref = refs[:tp], refs[tp], refs[tp + 1], refs[tp + 2]
+def up_kernel(part, col, *refs, tp, count, slots, slab):
+    x_refs, w_ref, out_ref, rows_ref = refs[: count * tp], refs[count * tp], refs[count * tp + 1], refs[count * tp + 2]
+    rows = x_refs[0].shape[0]
 
     @pl.when(pl.program_id(0) == 0)
     def _():
@@ -156,67 +157,76 @@
                 @pl.when(part[s] == j)
                 def _(s=s, j=j):
                     at = pl.multiple_of(col[s], slab)
-                    rows_ref[:, s * slab : (s + 1) * slab] = x_refs[j][:, pl.ds(at, slab)]
+                    for n in range(count):
+                        rows_ref[n * rows : (n + 1) * rows, s * slab : (s + 1) * slab] = x_refs[n * tp + j][
+                            :, pl.ds(at, slab)
+                        ]
 
     hidden = jnp.dot(rows_ref[...], w_ref[...], preferred_element_type=jnp.float32)
     positive = jnp.maximum(hidden, 0.0)
     out_ref[...] = (positive * positive).astype(jnp.bfloat16)
 
 
-def up_project(part, col, parts, weight, slots):
-    tp = len(parts)
-    rows, width = parts[0].shape
+def up_project(part, col, chunks, weight, slots):
+    count, tp = len(chunks), len(chunks[0])
+    rows, width = chunks[0][0].shape
     depth, units = weight.shape
     block = min(256, units)
     grid_spec = pltpu.PrefetchScalarGridSpec(
         num_scalar_prefetch=2,
         grid=(units // block,),
-        in_specs=[pl.BlockSpec((rows, width), lambda n, a, b: (0, 0))] * tp
+        in_specs=[pl.BlockSpec((rows, width), lambda n, a, b: (0, 0))] * (count * tp)
         + [pl.BlockSpec((depth, block), lambda n, a, b: (0, n))],
-        out_specs=pl.BlockSpec((rows, block), lambda n, a, b: (0, n)),
-        scratch_shapes=[pltpu.VMEM((rows, depth), jnp.bfloat16)],
+        out_specs=pl.BlockSpec((count * rows, block), lambda n, a, b: (0, n)),
+        scratch_shapes=[pltpu.VMEM((count * rows, depth), jnp.bfloat16)],
     )
     return pl.pallas_call(
-        functools.partial(up_kernel, tp=tp, slots=slots, slab=depth // slots),
+        functools.partial(up_kernel, tp=tp, count=count, slots=slots, slab=depth // slots),
         grid_spec=grid_spec,
-        out_shape=jax.ShapeDtypeStruct((rows, units), jnp.bfloat16),
+        out_shape=jax.ShapeDtypeStruct((count * rows, units), jnp.bfloat16),
         cost_estimate=pl.CostEstimate(
-            flops=2 * rows * depth * units, bytes_accessed=2 * depth * (units + rows), transcendentals=0
+            flops=2 * count * rows * depth * units,
+            bytes_accessed=2 * depth * (units + count * rows),
+            transcendentals=0,
         ),
-    )(part, col, *parts, weight)
-
-
-def down_kernel(part, col, x_ref, w_ref, *out_refs, slab):
-    s = pl.program_id(0)
-    result = jnp.dot(x_ref[...], w_ref[...], preferred_element_type=jnp.float32).astype(jnp.bfloat16)
-    for j, out_ref in enumerate(out_refs):
-
-        @pl.when(part[s] == j)
-        def _(out_ref=out_ref):
-            out_ref[:, pl.ds(pl.multiple_of(col[s], slab), slab)] = result
-
-
-def down_project(part, col, squared, weight, tp, slots):
+    )(part, col, *[piece for chunk in chunks for piece in chunk], weight)
+
+
+def down_kernel(part, col, x_ref, w_ref, *refs):
+    out_ref = refs[-1]
+    out_ref[0] = jnp.dot(x_ref[...], w_ref[...], preferred_element_type=jnp.float32).astype(jnp.bfloat16)
+
+
+def down_project(part, col, squared, weight, tp, slots, first, into):
     rows, units = squared.shape
     slab = weight.shape[1]
+    count = weight.shape[0] // units
     width = slab * slots // tp
     grid_spec = pltpu.PrefetchScalarGridSpec(
         num_scalar_prefetch=2,
-        grid=(slots,),
+        grid=(count,),
         in_specs=[
             pl.BlockSpec((rows, units), lambda s, a, b: (0, 0)),
             pl.BlockSpec((units, slab), lambda s, a, b: (s, 0)),
-        ],
-        out_specs=[pl.BlockSpec((rows, width), lambda s, a, b: (0, 0))] * tp,
+        ]
+        + ([] if into is None else [pl.BlockSpec(memory_space=pl.ANY)]),
+        out_specs=pl.BlockSpec((1, rows, slab), lambda s, a, b: (a[first + s], 0, b[first + s] // slab)),
     )
     return pl.pallas_call(
-        functools.partial(down_kernel, slab=slab),
+        down_kernel,
         grid_spec=grid_spec,
-        out_shape=[jax.ShapeDtypeStruct((rows, width), jnp.bfloat16)] * tp,
+        out_shape=jax.ShapeDtypeStruct((tp, rows, width), jnp.bfloat16),
+        input_output_aliases={} if into is None else {4: 0},
         cost_estimate=pl.CostEstimate(
-            flops=2 * rows * units * slab * slots, bytes_accessed=2 * units * (slab * slots + rows), transcendentals=0
+            flops=2 * rows * units * slab * count,
+            bytes_accessed=2 * units * (slab * count + rows),
+            transcendentals=0,
         ),
-    )(part, col, squared, weight)
+    )(part, col, squared, weight, *([] if into is None else [into]))
+
+
+def part_sum(pieces, offset, start, stop):
+    return sum(piece[offset + start : offset + stop].astype(jnp.float32) for piece in pieces)
 
 
 def spread(index, bits):
@@ -270,10 +280,12 @@
             for cs in groups:
                 stacked = pieces[cs[0]] if len(cs) == 1 else jnp.concatenate([pieces[c] for c in cs])
                 found += gather_wide(stacked)
-            return jnp.concatenate(found)
-
-        up_whole = gather_units(up_weight, 1)
-        down_whole = gather_units(down_weight, 0)
+            return found
+
+        up_whole = jnp.concatenate(gather_units(up_weight, 1))
+        down_found = gather_units(down_weight, 0)
+        late = slots - 2 * wide
+        down_early, down_late = jnp.concatenate(down_found[:late]), jnp.concatenate(down_found[late:])
 
         docs_near = jnp.stack([documents] + [swap(documents, near_mask[c]) for c in far])
         docs_all = jnp.concatenate([docs_near] + [swap(docs_near, wide_mask[m]) for m in range(1, wide)])
@@ -346,21 +358,44 @@
             low = c & -c
             via = chunks[c ^ low] if c != low else normed
             chunks[c] = swap(via, near_mask[low])
-        squared = []
-        for c in range(near):
-            chunk_parts = [chunks[c]] + [swap_tp(chunks[c], j) for j in range(1, tp)]
-            squared.append(up_project(part, col, chunk_parts, up_whole, slots))
+        parts_of = [[chunks[c]] + [swap_tp(chunks[c], j) for j in range(1, tp)] for c in range(near)]
         feed = [None] * near
-        for c in list(far)[::-1] + [0]:
-            pieces = down_project(part, col, squared[c], down_whole, tp, slots)
-            total = pieces[0].astype(jnp.float32)
-            for j in range(1, tp):
-                total = total + swap_tp(pieces[j], j).astype(jnp.float32)
-            feed[c] = total
+        for c in range(0, near, 2):
+            squared = up_project(part, col, parts_of[c : c + 2], up_whole, slots)
+            product = down_project(part, col, squared, down_early, tp, slots, 0, None)
+            product = down_project(part, col, squared, down_late, tp, slots, late, product)
+            heard = [product[0]] + [swap_tp(product[j], j) for j in range(1, tp)]
+            feed[c] = functools.partial(part_sum, heard, 0)
+            feed[c + 1] = functools.partial(part_sum, heard, rows)
+        if near == 4:
+            half, low, high = rows // 2, near_mask[1], near_mask[2]
+
+            def send(value, mask):
+                return swap(value.astype(jnp.bfloat16), mask).astype(jnp.float32)
+
+            def low_bits(value):
+                return value.astype(jnp.bfloat16)
+
+            three_a, three_b, two_b, two_a = lax.optimization_barrier(
+                (low_bits(feed[3](0, half)), low_bits(feed[3](half, rows)), low_bits(feed[2](half, rows)), feed[2](0, half))
+            )
+            low_3, high_3, high_2 = send(three_a, low), send(three_b, high), send(two_b, high)
+            one_a, one_b, own_a, own_b = lax.optimization_barrier(
+                (low_bits(feed[1](0, half)), feed[1](half, rows), feed[0](0, half), feed[0](half, rows))
+            )
+            low_1 = send(one_a, low)
+            mixed_a = low_bits(two_a + low_3)
+            high_a = send(mixed_a, high)
+            mixed_b = low_bits(one_b + high_3)
+            low_b = send(mixed_b, low)
+            top = stream[:half] + (own_a + low_1 + high_a)
+            bottom = stream[half:] + (own_b + high_2 + low_b)
+            return jnp.concatenate([top.astype(jnp.bfloat16), bottom.astype(jnp.bfloat16)])
+        feed = [one(0, rows) for one in feed]
         for c in list(far)[::-1]:
-            low = c & -c
-            arrived = swap(feed[c].astype(jnp.bfloat16), near_mask[low])
-            feed[c ^ low] = feed[c ^ low] + arrived.astype(jnp.float32)
+            bit = c & -c
+            arrived = swap(feed[c].astype(jnp.bfloat16), near_mask[bit])
+            feed[c ^ bit] = feed[c ^ bit] + arrived.astype(jnp.float32)
         return (stream + feed[0]).astype(jnp.bfloat16)
 
     return body

time: 879 us -> 843 us (0.959)
  starting transfers between devices: 70.6 us -> 170 us
  waiting for transfers between devices: 486 us -> 396 us
  Pallas kernels: 193 us -> 154 us
    ppermute x51 -> x54, starting transfers between devices: 69.4 us -> 169 us  [swap(): return lax.ppermute(value, 'sp', [(s, s ^ mask) for s in range(sp)])]
    ppermute x51 -> x54, waiting for transfers between devices: 486 us -> 396 us  [swap(): return lax.ppermute(value, 'sp', [(s, s ^ mask) for s in range(sp)])]
    pallas_call x8 -> x6, Pallas kernels: 149 us -> 111 us  [the longest x4 59.1 us: down_project(): pl.pallas_call(down_kernel, grid_spec=grid_spec, out_shape=jax.ShapeDtype...]
    convert_element_type x4 -> x3, other arithmetic: 17.5 us -> 4.44 us  [the longest x2 3 us: low_bits(): return value.astype(jnp.bfloat16)]
    unnamed x66 -> x67, local copies, waits for them, and re-layouts: 45.2 us -> 39.9 us
  transfers between devices with their start and end apart: 61 -> 62, of which waited for: 29 -> 27; matrix products, arithmetic and copies ran while one was open for 11% -> 10% of each run, Pallas kernels for 17% -> 12%
where the time goes in v3:
time: 843 us; the launch traced here: 832 us
  waiting for transfers between devices  396 us (47%)
  starting transfers between devices  170 us (20%)
  Pallas kernels  154 us (18%)
  local copies, waits for them, and re-layouts  79.6 us (9%)
  other arithmetic  22.7 us (3%)
    ppermute x54, waiting for transfers between devices, swap(): return lax.ppermute(value, 'sp', [(s, s ^ mask) for s in range(sp)])  396 us
    ppermute x54, starting transfers between devices, swap(): return lax.ppermute(value, 'sp', [(s, s ^ mask) for s in range(sp)])  169 us
    pallas_call x4, Pallas kernels, down_project(): pl.pallas_call(down_kernel, grid_spec=grid_spec, out_shape=jax.ShapeDtype...  59.1 us
    pallas_call x2, Pallas kernels, up_project(): pl.pallas_call(functools.partial(up_kernel, tp=tp, count=count, slots=slo...  52 us
    pallas_call x1, Pallas kernels, attend(): pl.pallas_call(functools.partial(attend_kernel, group=group, blocks=block...  43.4 us
    unnamed x67, local copies, waits for them, and re-layouts  39.9 us
  transfers between devices with their start and end apart: 62, of which 27 were waited for; matrix products, arithmetic and copies ran while one was open for 10% of the time, Pallas kernels for 12%

profile of v3, /device:TPU:0, one launch (start us, length us, event | category | flops | bytes accessed | tf_op | source)
XLA Modules:
  0.0 832.2 jit_solution(13738548638515787762)
XLA Ops:
  29.8 9.0 %collective-permute-done.8 = bf16[512,512]{1,0:T(8,128)(2,1)} collective-permute-done((bf16[512,512]{1,0:T(8,128)(2,1)}, bf16[512,512]{1,0:T(8,128)(2,1)}, u32[]{:S(2)}, u32[]{:S(2)}) %collective-permute-start.8) | collective-permute-done | bytes 524320 | tf_op jit(solution)/shard_map/ppermute | solution.py:243
  55.0 34.9 %collective-permute-done.10 = bf16[2048,256]{1,0:T(8,128)(2,1)} collective-permute-done((bf16[2048,256]{1,0:T(8,128)(2,1)}, bf16[2048,256]{1,0:T(8,128)(2,1)}, u32[]{:S(2)}, u32[]{:S(2)}) %collective-permute-start.10) | collective-permute-done | bytes 1048608 | tf_op jit(solution)/shard_map/ppermute | solution.py:243
  104.5 11.8 %collective-permute-done.11 = bf16[2048,256]{1,0:T(8,128)(2,1)} collective-permute-done((bf16[2048,256]{1,0:T(8,128)(2,1)}, bf16[2048,256]{1,0:T(8,128)(2,1)}, u32[]{:S(2)}, u32[]{:S(2)}) %collective-permute-start.11) | collective-permute-done | bytes 1048608 | tf_op jit(solution)/shard_map/ppermute | solution.py:243
  118.6 43.4 %attend.1 = bf16[2048,256]{1,0:T(8,128)(2,1)} custom-call(s32[128]{0:T(128)} %select_n.98.flags, bf16[2048,256]{1,0:T(8,128)(2,1)} %bitcast.98, bf16[16,512,256]{2,1,0:T(8,128)(2,1)} %bitcast.103, s32[8,1,512]{2,1,0:T(1,128)} %tile.8.qdoc_ref, s32[16,512,1]{2,1,0:T(8,128)} %copy.85.kdoc_ref), custom_call_target="tpu_custom_call" | custom-call | flops 8589934592 | bytes 6291456 | tf_op jit(solution)/shard_map/attend/pallas_call | solution.py:136
  174.6 16.6 %collective-permute-start.43 = (bf16[2048,256]{1,0:T(8,128)(2,1)}, bf16[2048,256]{1,0:T(8,128)(2,1)S(1)}, u32[]{:S(2)}, u32[]{:S(2)}) collective-permute-start(bf16[2048,256]{1,0:T(8,128)(2,1)} %get-tuple-element.43), channel_id=1, source_target_pairs={{0,4},{2,6},{4,0},{6,2},{8,12},{10,14},{12,8},{14,10},{16,20},{18,... | collective-permute-start | bytes 3145736 | tf_op jit(solution)/shard_map/ppermute | solution.py:243
  200.2 8.2 convolution_convert_fusion
  208.4 32.7 %collective-permute-done.27 = bf16[256,2048]{1,0:T(8,128)(2,1)S(1)} collective-permute-done((bf16[256,2048]{1,0:T(8,128)(2,1)}, bf16[256,2048]{1,0:T(8,128)(2,1)S(1)}, u32[]{:S(2)}, u32[]{:S(2)}) %collective-permute-start.27) | collective-permute-done | bytes 1048608 | tf_op jit(solution)/shard_map/ppermute | solution.py:243
  245.0 11.6 %collective-permute-done.35 = bf16[2048,256]{1,0:T(8,128)(2,1)S(1)} collective-permute-done((bf16[2048,256]{1,0:T(8,128)(2,1)}, bf16[2048,256]{1,0:T(8,128)(2,1)S(1)}, u32[]{:S(2)}, u32[]{:S(2)}) %collective-permute-start.35) | collective-permute-done | bytes 1048608 | tf_op jit(solution)/shard_map/ppermute | solution.py:243
  273.2 35.2 %collective-permute-done.31 = bf16[256,2048]{1,0:T(8,128)(2,1)S(1)} collective-permute-done((bf16[256,2048]{1,0:T(8,128)(2,1)S(1)}, bf16[256,2048]{1,0:T(8,128)(2,1)S(1)}, u32[]{:S(2)}, u32[]{:S(2)}) %collective-permute-start.31) | collective-permute-done | bytes 1048608 | tf_op jit(solution)/shard_map/ppermute | solution.py:243
  322.9 29.9 %collective-permute-done.39 = bf16[2048,256]{1,0:T(8,128)(2,1)S(1)} collective-permute-done((bf16[2048,256]{1,0:T(8,128)(2,1)S(1)}, bf16[2048,256]{1,0:T(8,128)(2,1)S(1)}, u32[]{:S(2)}, u32[]{:S(2)}) %collective-permute-start.39) | collective-permute-done | bytes 1048608 | tf_op jit(solution)/shard_map/ppermute | solution.py:243
  352.8 9.7 %collective-permute-done.28 = bf16[256,2048]{1,0:T(8,128)(2,1)S(1)} collective-permute-done((bf16[256,2048]{1,0:T(8,128)(2,1)S(1)}, bf16[256,2048]{1,0:T(8,128)(2,1)S(1)}, u32[]{:S(2)}, u32[]{:S(2)}) %collective-permute-start.28) | collective-permute-done | bytes 1048608 | tf_op jit(solution)/shard_map/ppermute | solution.py:243
  366.1 47.9 %collective-permute-done.29 = bf16[256,2048]{1,0:T(8,128)(2,1)S(1)} collective-permute-done((bf16[256,2048]{1,0:T(8,128)(2,1)S(1)}, bf16[256,2048]{1,0:T(8,128)(2,1)S(1)}, u32[]{:S(2)}, u32[]{:S(2)}) %collective-permute-start.29) | collective-permute-done | bytes 1048608 | tf_op jit(solution)/shard_map/ppermute | solution.py:243
  414.1 22.1 %collective-permute-start.26 = (bf16[256,2048]{1,0:T(8,128)(2,1)S(1)}, bf16[256,2048]{1,0:T(8,128)(2,1)S(1)}, u32[]{:S(2)}, u32[]{:S(2)}) collective-permute-start(bf16[256,2048]{1,0:T(8,128)(2,1)S(1)} %collective-permute-done.25), channel_id=1, source_target_pairs={{0,4},{2,6},{4,0},{6,2},{8,12},{10,14},{12,8},{14,10},{16,20},{18,... | collective-permute-start | bytes 3145736 | tf_op jit(solution)/shard_map/ppermute | solution.py:243
  436.6 30.7 %collective-permute-start.52 = (bf16[512,2048]{1,0:T(8,128)(2,1)S(1)}, bf16[512,2048]{1,0:T(8,128)(2,1)}, u32[]{:S(2)}, u32[]{:S(2)}) collective-permute-start(bf16[512,2048]{1,0:T(8,128)(2,1)S(1)} %multiply_convert_fusion.refs_0_), channel_id=1, source_target_pairs={{0,8},{2,10},{4,12},{6,14},{8,0},{10,2},{12,4},{14,6},{16,24},{18,... | collective-permute-start | bytes 6291464 | tf_op jit(solution)/shard_map/ppermute | solution.py:243
  469.3 12.3 %collective-permute-done.48 = bf16[2048,256]{1,0:T(8,128)(2,1)S(1)} collective-permute-done((bf16[2048,256]{1,0:T(8,128)(2,1)S(1)}, bf16[2048,256]{1,0:T(8,128)(2,1)S(1)}, u32[]{:S(2)}, u32[]{:S(2)}) %collective-permute-start.48) | collective-permute-done | bytes 1048608 | tf_op jit(solution)/shard_map/ppermute | solution.py:243
  485.0 15.5 %collective-permute-done.33 = bf16[256,2048]{1,0:T(8,128)(2,1)S(1)} collective-permute-done((bf16[256,2048]{1,0:T(8,128)(2,1)S(1)}, bf16[256,2048]{1,0:T(8,128)(2,1)S(1)}, u32[]{:S(2)}, u32[]{:S(2)}) %collective-permute-start.33) | collective-permute-done | bytes 1048608 | tf_op jit(solution)/shard_map/ppermute | solution.py:243
  507.6 19.0 %collective-permute-start.38 = (bf16[2048,256]{1,0:T(8,128)(2,1)S(1)}, bf16[2048,256]{1,0:T(8,128)(2,1)S(1)}, u32[]{:S(2)}, u32[]{:S(2)}) collective-permute-start(bf16[2048,256]{1,0:T(8,128)(2,1)S(1)} %collective-permute-done.37), channel_id=1, source_target_pairs={{0,4},{2,6},{4,0},{6,2},{8,12},{10,14},{12,8},{14,10},{16,20},{18,... | collective-permute-start | bytes 3145736 | tf_op jit(solution)/shard_map/ppermute | solution.py:243
  532.3 12.4 %collective-permute-done.41 = bf16[2048,256]{1,0:T(8,128)(2,1)S(1)} collective-permute-done((bf16[2048,256]{1,0:T(8,128)(2,1)S(1)}, bf16[2048,256]{1,0:T(8,128)(2,1)S(1)}, u32[]{:S(2)}, u32[]{:S(2)}) %collective-permute-start.41) | collective-permute-done | bytes 1048608 | tf_op jit(solution)/shard_map/ppermute | solution.py:243
  544.8 19.5 %collective-permute-done.52.refs_0_ = bf16[512,2048]{1,0:T(8,128)(2,1)} collective-permute-done((bf16[512,2048]{1,0:T(8,128)(2,1)S(1)}, bf16[512,2048]{1,0:T(8,128)(2,1)}, u32[]{:S(2)}, u32[]{:S(2)}) %collective-permute-start.52) | collective-permute-done | bytes 2097184 | tf_op jit(solution)/shard_map/ppermute | solution.py:243
  577.9 18.7 %collective-permute-done.42 = bf16[2048,256]{1,0:T(8,128)(2,1)S(1)} collective-permute-done((bf16[2048,256]{1,0:T(8,128)(2,1)S(1)}, bf16[2048,256]{1,0:T(8,128)(2,1)S(1)}, u32[]{:S(2)}, u32[]{:S(2)}) %collective-permute-start.42) | collective-permute-done | bytes 1048608 | tf_op jit(solution)/shard_map/ppermute | solution.py:243
  597.6 21.1 %collective-permute-done.49 = bf16[2048,256]{1,0:T(8,128)(2,1)S(1)} collective-permute-done((bf16[2048,256]{1,0:T(8,128)(2,1)S(1)}, bf16[2048,256]{1,0:T(8,128)(2,1)S(1)}, u32[]{:S(2)}, u32[]{:S(2)}) %collective-permute-start.49) | collective-permute-done | bytes 1048608 | tf_op jit(solution)/shard_map/ppermute | solution.py:243
  624.8 26.1 %shard_map.109.x_ref = bf16[1024,2048]{1,0:T(8,128)(2,1)} custom-call(s32[16]{0:T(128)} %get-tuple-element.82.part, s32[16]{0:T(128)} %get-tuple-element.81.col, bf16[512,2048]{1,0:T(8,128)(2,1)} %copy-done.6, bf16[512,2048]{1,0:T(8,128)(2,1)} %copy-done.13, bf16[512,2048]{1,0:T(8,128)(2,1)} %copy-done.12, bf16[512,2048]{1,0:T(8,128)(2,1)} %copy-done.14, ...), custom_call_target="tpu_custom_call" | custom-call | flops 17179869184 | bytes 25165824 | tf_op jit(solution)/shard_map/pallas_call | solution.py:183
  650.8 14.7 %shard_map.110.refs_0_ = bf16[2,1024,2048]{2,1,0:T(8,128)(2,1)} custom-call(s32[16]{0:T(128)} %get-tuple-element.82.part, s32[16]{0:T(128)} %get-tuple-element.81.col, bf16[1024,2048]{1,0:T(8,128)(2,1)} %shard_map.109.x_ref, bf16[16384,256]{1,0:T(8,128)(2,1)} %copy-done.8), custom_call_target="tpu_custom_call" | custom-call | flops 8589934592 | bytes 12582912 | tf_op jit(solution)/shard_map/pallas_call | solution.py:215
  665.6 25.9 %shard_map.112.x_ref = bf16[1024,2048]{1,0:T(8,128)(2,1)} custom-call(s32[16]{0:T(128)} %get-tuple-element.82.part, s32[16]{0:T(128)} %get-tuple-element.81.col, bf16[512,2048]{1,0:T(8,128)(2,1)} %collective-permute-done.52.refs_0_, bf16[512,2048]{1,0:T(8,128)(2,1)} %collective-permute-done.53.refs_1_, bf16[512,2048]{1,0:T(8,128)(2,1)} %collective-permute-done.54.refs_2_, ...), custom_call_target="tpu_custom_call" | custom-call | flops 17179869184 | bytes 25165824 | tf_op jit(solution)/shard_map/pallas_call | solution.py:183
  691.5 14.7 %shard_map.113.refs_0_ = bf16[2,1024,2048]{2,1,0:T(8,128)(2,1)} custom-call(s32[16]{0:T(128)} %get-tuple-element.82.part, s32[16]{0:T(128)} %get-tuple-element.81.col, bf16[1024,2048]{1,0:T(8,128)(2,1)} %shard_map.112.x_ref, bf16[16384,256]{1,0:T(8,128)(2,1)} %copy-done.8), custom_call_target="tpu_custom_call" | custom-call | flops 8589934592 | bytes 12582912 | tf_op jit(solution)/shard_map/pallas_call | solution.py:215
  706.2 14.7 %shard_map.114 = bf16[2,1024,2048]{2,1,0:T(8,128)(2,1)} custom-call(s32[16]{0:T(128)} %get-tuple-element.82.part, s32[16]{0:T(128)} %get-tuple-element.81.col, bf16[1024,2048]{1,0:T(8,128)(2,1)} %shard_map.112.x_ref, bf16[16384,256]{1,0:T(8,128)(2,1)} %constant_dynamic-update-slice_fusion.24.w_ref, ...), custom_call_target="tpu_custom_call", output_to_operand_aliasing={{}: (4, {})} | custom-call | flops 8589934592 | bytes 12582912 | tf_op jit(solution)/shard_map/pallas_call | solution.py:215
  725.7 14.9 %shard_map.111 = bf16[2,1024,2048]{2,1,0:T(8,128)(2,1)} custom-call(s32[16]{0:T(128)} %get-tuple-element.82.part, s32[16]{0:T(128)} %get-tuple-element.81.col, bf16[1024,2048]{1,0:T(8,128)(2,1)} %shard_map.109.x_ref, bf16[16384,256]{1,0:T(8,128)(2,1)} %constant_dynamic-update-slice_fusion.24.w_ref, ...), custom_call_target="tpu_custom_call", output_to_operand_aliasing={{}: (4, {})} | custom-call | flops 8589934592 | bytes 12582912 | tf_op jit(solution)/shard_map/pallas_call | solution.py:215
  751.7 8.7 %collective-permute-start.60 = (bf16[256,2048]{1,0:T(8,128)(2,1)}, bf16[256,2048]{1,0:T(8,128)(2,1)}, u32[]{:S(2)}, u32[]{:S(2)}) collective-permute-start(bf16[256,2048]{1,0:T(8,128)(2,1)} %get-tuple-element.20), channel_id=1, source_target_pairs={{0,8},{2,10},{4,12},{6,14},{8,0},{10,2},{12,4},{14,6},{16,24},{18,... | collective-permute-start | bytes 3145736 | tf_op jit(solution)/shard_map/ppermute | solution.py:243
  764.4 13.1 %collective-permute-done.57 = bf16[256,2048]{1,0:T(8,128)(2,1)} collective-permute-done((bf16[256,2048]{1,0:T(8,128)(2,1)}, bf16[256,2048]{1,0:T(8,128)(2,1)}, u32[]{:S(2)}, u32[]{:S(2)}) %collective-permute-start.57) | collective-permute-done | bytes 1048608 | tf_op jit(solution)/shard_map/ppermute | solution.py:243
  779.0 8.4 %collective-permute-start.58 = (bf16[256,2048]{1,0:T(8,128)(2,1)S(1)}, bf16[256,2048]{1,0:T(8,128)(2,1)S(1)}, u32[]{:S(2)}, u32[]{:S(2)}) collective-permute-start(bf16[256,2048]{1,0:T(8,128)(2,1)S(1)} %add_convert_fusion.1), channel_id=1, source_target_pairs={{0,8},{2,10},{4,12},{6,14},{8,0},{10,2},{12,4},{14,6},{16,24},{18,... | collective-permute-start | bytes 3145736 | tf_op jit(solution)/shard_map/ppermute | solution.py:243
  789.8 10.0 %collective-permute-done.51 = bf16[256,2048]{1,0:T(8,128)(2,1)S(1)} collective-permute-done((bf16[256,2048]{1,0:T(8,128)(2,1)}, bf16[256,2048]{1,0:T(8,128)(2,1)S(1)}, u32[]{:S(2)}, u32[]{:S(2)}) %collective-permute-start.51) | collective-permute-done | bytes 1048608 | tf_op jit(solution)/shard_map/ppermute | solution.py:243
  807.0 22.0 %collective-permute-done.58 = bf16[256,2048]{1,0:T(8,128)(2,1)S(1)} collective-permute-done((bf16[256,2048]{1,0:T(8,128)(2,1)S(1)}, bf16[256,2048]{1,0:T(8,128)(2,1)S(1)}, u32[]{:S(2)}, u32[]{:S(2)}) %collective-permute-start.58) | collective-permute-done | bytes 1048608 | tf_op jit(solution)/shard_map/ppermute | solution.py:243
  (236 shorter events, 196.1 us)
Async XLA Ops:
  41.7 48.2 %collective-permute-start.10 = (bf16[2048,256]{1,0:T(8,128)(2,1)}, bf16[2048,256]{1,0:T(8,128)(2,1)}, u32[]{:S(2)}, u32[]{:S(2)}) collective-permute-start(bf16[2048,256]{1,0:T(8,128)(2,1)} %pad_maximum_fusion.3), channel_id=1, source_target_pairs={{0,16},{2,18},{4,20},{6,22},{8,24},{10,26},{12,28},{14,30},{16,0},... | collective-permute-start | bytes 3145736 | tf_op jit(solution)/shard_map/ppermute | solution.py:243
  46.8 53.1 %collective-permute-start.9 = (bf16[2048,256]{1,0:T(8,128)(2,1)}, bf16[2048,256]{1,0:T(8,128)(2,1)}, u32[]{:S(2)}, u32[]{:S(2)}) collective-permute-start(bf16[2048,256]{1,0:T(8,128)(2,1)} %pad_maximum_fusion.3), channel_id=1, source_target_pairs={{0,4},{2,6},{4,0},{6,2},{8,12},{10,14},{12,8},{14,10},{16,20},{18,... | collective-permute-start | bytes 3145736 | tf_op jit(solution)/shard_map/ppermute | solution.py:243
  92.0 75.6 %collective-permute-start.20 = (bf16[256,2048]{1,0:T(8,128)(2,1)}, bf16[256,2048]{1,0:T(8,128)(2,1)}, u32[]{:S(2)}, u32[]{:S(2)}) collective-permute-start(bf16[256,2048]{1,0:T(8,128)(2,1)} %get-tuple-element.47), channel_id=1, source_target_pairs={{0,4},{2,6},{4,0},{6,2},{8,12},{10,14},{12,8},{14,10},{16,20},{18,... | collective-permute-start | bytes 3145736 | tf_op jit(solution)/shard_map/ppermute | solution.py:243
  92.6 101.7 %collective-permute-start.21 = (bf16[256,2048]{1,0:T(8,128)(2,1)}, bf16[256,2048]{1,0:T(8,128)(2,1)}, u32[]{:S(2)}, u32[]{:S(2)}) collective-permute-start(bf16[256,2048]{1,0:T(8,128)(2,1)} %get-tuple-element.47), channel_id=1, source_target_pairs={{0,16},{2,18},{4,20},{6,22},{8,24},{10,26},{12,28},{14,30},{16,0},... | collective-permute-start | bytes 3145736 | tf_op jit(solution)/shard_map/ppermute | solution.py:243
  92.6 103.7 %collective-permute-start.23 = (bf16[256,2048]{1,0:T(8,128)(2,1)}, bf16[256,2048]{1,0:T(8,128)(2,1)}, u32[]{:S(2)}, u32[]{:S(2)}) collective-permute-start(bf16[256,2048]{1,0:T(8,128)(2,1)} %get-tuple-element.45), channel_id=1, source_target_pairs={{0,2},{2,0},{4,6},{6,4},{8,10},{10,8},{12,14},{14,12},{16,18},{18,... | collective-permute-start | bytes 3145736 | tf_op jit(solution)/shard_map/ppermute | solution.py:243
  174.6 85.3 %collective-permute-start.43 = (bf16[2048,256]{1,0:T(8,128)(2,1)}, bf16[2048,256]{1,0:T(8,128)(2,1)S(1)}, u32[]{:S(2)}, u32[]{:S(2)}) collective-permute-start(bf16[2048,256]{1,0:T(8,128)(2,1)} %get-tuple-element.43), channel_id=1, source_target_pairs={{0,4},{2,6},{4,0},{6,2},{8,12},{10,14},{12,8},{14,10},{16,20},{18,... | collective-permute-start | bytes 3145736 | tf_op jit(solution)/shard_map/ppermute | solution.py:243
  192.9 67.6 %collective-permute-start.44 = (bf16[2048,256]{1,0:T(8,128)(2,1)}, bf16[2048,256]{1,0:T(8,128)(2,1)S(1)}, u32[]{:S(2)}, u32[]{:S(2)}) collective-permute-start(bf16[2048,256]{1,0:T(8,128)(2,1)} %get-tuple-element.43), channel_id=1, source_target_pairs={{0,16},{2,18},{4,20},{6,22},{8,24},{10,26},{12,28},{14,30},{16,0},... | collective-permute-start | bytes 3145736 | tf_op jit(solution)/shard_map/ppermute | solution.py:243
  193.6 47.5 %collective-permute-start.27 = (bf16[256,2048]{1,0:T(8,128)(2,1)}, bf16[256,2048]{1,0:T(8,128)(2,1)S(1)}, u32[]{:S(2)}, u32[]{:S(2)}) collective-permute-start(bf16[256,2048]{1,0:T(8,128)(2,1)} %get-tuple-element.48), channel_id=1, source_target_pairs={{0,8},{2,10},{4,12},{6,14},{8,0},{10,2},{12,4},{14,6},{16,24},{18,... | collective-permute-start | bytes 3145736 | tf_op jit(solution)/shard_map/ppermute | solution.py:243
  194.3 62.2 %collective-permute-start.35 = (bf16[2048,256]{1,0:T(8,128)(2,1)}, bf16[2048,256]{1,0:T(8,128)(2,1)S(1)}, u32[]{:S(2)}, u32[]{:S(2)}) collective-permute-start(bf16[2048,256]{1,0:T(8,128)(2,1)} %get-tuple-element.41), channel_id=1, source_target_pairs={{0,8},{2,10},{4,12},{6,14},{8,0},{10,2},{12,4},{14,6},{16,24},{18,... | collective-permute-start | bytes 3145736 | tf_op jit(solution)/shard_map/ppermute | solution.py:243
  196.3 68.7 %collective-permute-start.22 = (bf16[256,2048]{1,0:T(8,128)(2,1)}, bf16[256,2048]{1,0:T(8,128)(2,1)S(1)}, u32[]{:S(2)}, u32[]{:S(2)}) collective-permute-start(bf16[256,2048]{1,0:T(8,128)(2,1)} %collective-permute-done.21), channel_id=1, source_target_pairs={{0,4},{2,6},{4,0},{6,2},{8,12},{10,14},{12,8},{14,10},{16,20},{18,... | collective-permute-start | bytes 3145736 | tf_op jit(solution)/shard_map/ppermute | solution.py:243
  256.6 64.9 %collective-permute-start.15 = (bf16[512,2048]{1,0:T(8,128)(2,1)S(1)}, bf16[512,2048]{1,0:T(8,128)(2,1)S(1)}, u32[]{:S(2)}, u32[]{:S(2)}) collective-permute-start(bf16[512,2048]{1,0:T(8,128)(2,1)S(1)} %constant_dynamic-slice_fusion.8), channel_id=1, source_target_pairs={{0,1},{1,0},{2,3},{3,2},{4,5},{5,4},{6,7},{7,6},{8,9},{9,8},{10,11... | collective-permute-start | bytes 6291464 | tf_op jit(solution)/shard_map/ppermute | solution.py:246
  259.9 48.5 %collective-permute-start.31 = (bf16[256,2048]{1,0:T(8,128)(2,1)S(1)}, bf16[256,2048]{1,0:T(8,128)(2,1)S(1)}, u32[]{:S(2)}, u32[]{:S(2)}) collective-permute-start(bf16[256,2048]{1,0:T(8,128)(2,1)S(1)} %get-tuple-element.44), channel_id=1, source_target_pairs={{0,10},{2,8},{4,14},{6,12},{8,2},{10,0},{12,6},{14,4},{16,26},{18,... | collective-permute-start | bytes 3145736 | tf_op jit(solution)/shard_map/ppermute | solution.py:243
  260.4 50.9 %collective-permute-start.25 = (bf16[256,2048]{1,0:T(8,128)(2,1)}, bf16[256,2048]{1,0:T(8,128)(2,1)S(1)}, u32[]{:S(2)}, u32[]{:S(2)}) collective-permute-start(bf16[256,2048]{1,0:T(8,128)(2,1)} %collective-permute-done.23), channel_id=1, source_target_pairs={{0,16},{2,18},{4,20},{6,22},{8,24},{10,26},{12,28},{14,30},{16,0},... | collective-permute-start | bytes 3145736 | tf_op jit(solution)/shard_map/ppermute | solution.py:243
  265.0 51.0 %collective-permute-start.45 = (bf16[2048,256]{1,0:T(8,128)(2,1)S(1)}, bf16[2048,256]{1,0:T(8,128)(2,1)S(1)}, u32[]{:S(2)}, u32[]{:S(2)}) collective-permute-start(bf16[2048,256]{1,0:T(8,128)(2,1)S(1)} %collective-permute-done.44), channel_id=1, source_target_pairs={{0,4},{2,6},{4,0},{6,2},{8,12},{10,14},{12,8},{14,10},{16,20},{18,... | collective-permute-start | bytes 3145736 | tf_op jit(solution)/shard_map/ppermute | solution.py:243
  267.2 54.2 %collective-permute-start.46 = (bf16[2048,256]{1,0:T(8,128)(2,1)S(1)}, bf16[2048,256]{1,0:T(8,128)(2,1)S(1)}, u32[]{:S(2)}, u32[]{:S(2)}) collective-permute-start(bf16[2048,256]{1,0:T(8,128)(2,1)S(1)} %get-tuple-element.39), channel_id=1, source_target_pairs={{0,2},{2,0},{4,6},{6,4},{8,10},{10,8},{12,14},{14,12},{16,18},{18,... | collective-permute-start | bytes 3145736 | tf_op jit(solution)/shard_map/ppermute | solution.py:243
  311.3 53.2 %collective-permute-start.36 = (bf16[2048,256]{1,0:T(8,128)(2,1)S(1)}, bf16[2048,256]{1,0:T(8,128)(2,1)S(1)}, u32[]{:S(2)}, u32[]{:S(2)}) collective-permute-start(bf16[2048,256]{1,0:T(8,128)(2,1)S(1)} %collective-permute-done.35), channel_id=1, source_target_pairs={{0,4},{2,6},{4,0},{6,2},{8,12},{10,14},{12,8},{14,10},{16,20},{18,... | collective-permute-start | bytes 3145736 | tf_op jit(solution)/shard_map/ppermute | solution.py:243
  321.5 92.6 %collective-permute-start.29 = (bf16[256,2048]{1,0:T(8,128)(2,1)S(1)}, bf16[256,2048]{1,0:T(8,128)(2,1)S(1)}, u32[]{:S(2)}, u32[]{:S(2)}) collective-permute-start(bf16[256,2048]{1,0:T(8,128)(2,1)S(1)} %collective-permute-done.27), channel_id=1, source_target_pairs={{0,16},{2,18},{4,20},{6,22},{8,24},{10,26},{12,28},{14,30},{16,0},... | collective-permute-start | bytes 3145736 | tf_op jit(solution)/shard_map/ppermute | solution.py:243
  321.5 92.6 %collective-permute-start.32 = (bf16[256,2048]{1,0:T(8,128)(2,1)S(1)}, bf16[256,2048]{1,0:T(8,128)(2,1)S(1)}, u32[]{:S(2)}, u32[]{:S(2)}) collective-permute-start(bf16[256,2048]{1,0:T(8,128)(2,1)S(1)} %collective-permute-done.31), channel_id=1, source_target_pairs={{0,4},{2,6},{4,0},{6,2},{8,12},{10,14},{12,8},{14,10},{16,20},{18,... | collective-permute-start | bytes 3145736 | tf_op jit(solution)/shard_map/ppermute | solution.py:243
  352.8 83.8 %collective-permute-start.37 = (bf16[2048,256]{1,0:T(8,128)(2,1)S(1)}, bf16[2048,256]{1,0:T(8,128)(2,1)S(1)}, u32[]{:S(2)}, u32[]{:S(2)}) collective-permute-start(bf16[2048,256]{1,0:T(8,128)(2,1)S(1)} %collective-permute-done.35), channel_id=1, source_target_pairs={{0,16},{2,18},{4,20},{6,22},{8,24},{10,26},{12,28},{14,30},{16,0},... | collective-permute-start | bytes 3145736 | tf_op jit(solution)/shard_map/ppermute | solution.py:243
  362.5 104.8 %collective-permute-start.47 = (bf16[2048,256]{1,0:T(8,128)(2,1)S(1)}, bf16[2048,256]{1,0:T(8,128)(2,1)S(1)}, u32[]{:S(2)}, u32[]{:S(2)}) collective-permute-start(bf16[2048,256]{1,0:T(8,128)(2,1)S(1)} %collective-permute-done.46), channel_id=1, source_target_pairs={{0,4},{2,6},{4,0},{6,2},{8,12},{10,14},{12,8},{14,10},{16,20},{18,... | collective-permute-start | bytes 3145736 | tf_op jit(solution)/shard_map/ppermute | solution.py:243
  365.7 115.9 %collective-permute-start.48 = (bf16[2048,256]{1,0:T(8,128)(2,1)S(1)}, bf16[2048,256]{1,0:T(8,128)(2,1)S(1)}, u32[]{:S(2)}, u32[]{:S(2)}) collective-permute-start(bf16[2048,256]{1,0:T(8,128)(2,1)S(1)} %collective-permute-done.46), channel_id=1, source_target_pairs={{0,16},{2,18},{4,20},{6,22},{8,24},{10,26},{12,28},{14,30},{16,0},... | collective-permute-start | bytes 3145736 | tf_op jit(solution)/shard_map/ppermute | solution.py:243
  414.1 86.4 %collective-permute-start.33 = (bf16[256,2048]{1,0:T(8,128)(2,1)S(1)}, bf16[256,2048]{1,0:T(8,128)(2,1)S(1)}, u32[]{:S(2)}, u32[]{:S(2)}) collective-permute-start(bf16[256,2048]{1,0:T(8,128)(2,1)S(1)} %collective-permute-done.31), channel_id=1, source_target_pairs={{0,16},{2,18},{4,20},{6,22},{8,24},{10,26},{12,28},{14,30},{16,0},... | collective-permute-start | bytes 3145736 | tf_op jit(solution)/shard_map/ppermute | solution.py:243
  414.1 67.6 %collective-permute-start.26 = (bf16[256,2048]{1,0:T(8,128)(2,1)S(1)}, bf16[256,2048]{1,0:T(8,128)(2,1)S(1)}, u32[]{:S(2)}, u32[]{:S(2)}) collective-permute-start(bf16[256,2048]{1,0:T(8,128)(2,1)S(1)} %collective-permute-done.25), channel_id=1, source_target_pairs={{0,4},{2,6},{4,0},{6,2},{8,12},{10,14},{12,8},{14,10},{16,20},{18,... | collective-permute-start | bytes 3145736 | tf_op jit(solution)/shard_map/ppermute | solution.py:243
  436.6 127.7 %collective-permute-start.52 = (bf16[512,2048]{1,0:T(8,128)(2,1)S(1)}, bf16[512,2048]{1,0:T(8,128)(2,1)}, u32[]{:S(2)}, u32[]{:S(2)}) collective-permute-start(bf16[512,2048]{1,0:T(8,128)(2,1)S(1)} %multiply_convert_fusion.refs_0_), channel_id=1, source_target_pairs={{0,8},{2,10},{4,12},{6,14},{8,0},{10,2},{12,4},{14,6},{16,24},{18,... | collective-permute-start | bytes 6291464 | tf_op jit(solution)/shard_map/ppermute | solution.py:243
  467.3 98.4 %collective-permute-start.18 = (bf16[512,2048]{1,0:T(8,128)(2,1)S(1)}, bf16[512,2048]{1,0:T(8,128)(2,1)S(1)}, u32[]{:S(2)}, u32[]{:S(2)}) collective-permute-start(bf16[512,2048]{1,0:T(8,128)(2,1)S(1)} %multiply_convert_fusion.refs_0_), channel_id=1, source_target_pairs={{0,2},{2,0},{4,6},{6,4},{8,10},{10,8},{12,14},{14,12},{16,18},{18,... | collective-permute-start | bytes 6291464 | tf_op jit(solution)/shard_map/ppermute | solution.py:243
  481.7 48.4 %collective-permute-start.30 = (bf16[256,2048]{1,0:T(8,128)(2,1)S(1)}, bf16[256,2048]{1,0:T(8,128)(2,1)S(1)}, u32[]{:S(2)}, u32[]{:S(2)}) collective-permute-start(bf16[256,2048]{1,0:T(8,128)(2,1)S(1)} %collective-permute-done.29), channel_id=1, source_target_pairs={{0,4},{2,6},{4,0},{6,2},{8,12},{10,14},{12,8},{14,10},{16,20},{18,... | collective-permute-start | bytes 3145736 | tf_op jit(solution)/shard_map/ppermute | solution.py:243
  507.6 60.3 %collective-permute-start.38 = (bf16[2048,256]{1,0:T(8,128)(2,1)S(1)}, bf16[2048,256]{1,0:T(8,128)(2,1)S(1)}, u32[]{:S(2)}, u32[]{:S(2)}) collective-permute-start(bf16[2048,256]{1,0:T(8,128)(2,1)S(1)} %collective-permute-done.37), channel_id=1, source_target_pairs={{0,4},{2,6},{4,0},{6,2},{8,12},{10,14},{12,8},{14,10},{16,20},{18,... | collective-permute-start | bytes 3145736 | tf_op jit(solution)/shard_map/ppermute | solution.py:243
  544.8 74.7 %collective-permute-start.17 = (bf16[512,2048]{1,0:T(8,128)(2,1)S(1)}, bf16[512,2048]{1,0:T(8,128)(2,1)S(1)}, u32[]{:S(2)}, u32[]{:S(2)}) collective-permute-start(bf16[512,2048]{1,0:T(8,128)(2,1)S(1)} %multiply_convert_fusion.refs_0_), channel_id=1, source_target_pairs={{0,1},{1,0},{2,3},{3,2},{4,5},{5,4},{6,7},{7,6},{8,9},{9,8},{10,11... | collective-permute-start | bytes 6291464 | tf_op jit(solution)/shard_map/ppermute | solution.py:246
  564.3 54.7 %collective-permute-start.54 = (bf16[512,2048]{1,0:T(8,128)(2,1)}, bf16[512,2048]{1,0:T(8,128)(2,1)}, u32[]{:S(2)}, u32[]{:S(2)}) collective-permute-start(bf16[512,2048]{1,0:T(8,128)(2,1)} %collective-permute-done.52.refs_0_), channel_id=1, source_target_pairs={{0,2},{2,0},{4,6},{6,4},{8,10},{10,8},{12,14},{14,12},{16,18},{18,... | collective-permute-start | bytes 6291464 | tf_op jit(solution)/shard_map/ppermute | solution.py:243
  565.7 56.4 %collective-permute-start.19 = (bf16[512,2048]{1,0:T(8,128)(2,1)S(1)}, bf16[512,2048]{1,0:T(8,128)(2,1)S(1)}, u32[]{:S(2)}, u32[]{:S(2)}) collective-permute-start(bf16[512,2048]{1,0:T(8,128)(2,1)S(1)} %collective-permute-done.18.refs_2_), channel_id=1, source_target_pairs={{0,1},{1,0},{2,3},{3,2},{4,5},{5,4},{6,7},{7,6},{8,9},{9,8},{10,11... | collective-permute-start | bytes 6291464 | tf_op jit(solution)/shard_map/ppermute | solution.py:246
  618.9 46.7 %collective-permute-start.53 = (bf16[512,2048]{1,0:T(8,128)(2,1)}, bf16[512,2048]{1,0:T(8,128)(2,1)}, u32[]{:S(2)}, u32[]{:S(2)}) collective-permute-start(bf16[512,2048]{1,0:T(8,128)(2,1)} %collective-permute-done.52.refs_0_), channel_id=1, source_target_pairs={{0,1},{1,0},{2,3},{3,2},{4,5},{5,4},{6,7},{7,6},{8,9},{9,8},{10,11... | collective-permute-start | bytes 6291464 | tf_op jit(solution)/shard_map/ppermute | solution.py:246
  779.0 50.0 %collective-permute-start.58 = (bf16[256,2048]{1,0:T(8,128)(2,1)S(1)}, bf16[256,2048]{1,0:T(8,128)(2,1)S(1)}, u32[]{:S(2)}, u32[]{:S(2)}) collective-permute-start(bf16[256,2048]{1,0:T(8,128)(2,1)S(1)} %add_convert_fusion.1), channel_id=1, source_target_pairs={{0,8},{2,10},{4,12},{6,14},{8,0},{10,2},{12,4},{14,6},{16,24},{18,... | collective-permute-start | bytes 3145736 | tf_op jit(solution)/shard_map/ppermute | solution.py:243
  (48 other events, 1603.8 us)
